TPU v7x, 32 devices: a whole 2x2x4 slice. The times are simulated.
32 devices in a mesh: sp: 8 (over z, y), tp: 4 (over x, core).
Axes of the slice: x: 2, y: 2, z: 4, core: 2. Of those that a mesh axis runs over, the one named last changes fastest.
Arguments:
- queries: bfloat16 [4096, 1024], P('sp', 'tp'), may hold values from -200 to 200
- keys: bfloat16 [4096, 1024], P('sp', 'tp'), may hold values from -6 to 6
- values: bfloat16 [4096, 1024], P('sp', 'tp'), may hold values from -24 to 24
- cum_gate: float32 [4096, 8], P('sp', 'tp'), may hold values from -414 to 0, as said below
- residual: bfloat16 [4096, 2048], P(('sp', 'tp')), may hold values from -1.5 to 1.5
- w_out: bfloat16 [1024, 2048], replicated, may hold values from -0.1875 to 0.1875
- gain: float32 [2048], replicated, may hold values from 0.1 to 1.9
- w_up: bfloat16 [2048, 8192], P('sp', 'tp'), may hold values from -0.125 to 0.125
- w_down: bfloat16 [8192, 2048], P('tp', 'sp'), may hold values from -0.0625 to 0.0625
Outputs:
- output: bfloat16 [4096, 2048], P(('sp', 'tp'))
Inputs may be any that keep to these rules, and one draw needn't show every extreme that they name: Within each head, cum_gate never rises from one position to the next.
All inputs are finite; a program needn't handle non-finite values.
Results may differ from a plain program's by a relative error of at most 0.022.
Values may be sent and summed in bfloat16 or wider, within the bound.
A program may use at most 128 MiB of HBM per device.

v0:
```python
import functools
import math

import jax
import jax.numpy as jnp
from jax import lax
from jax.experimental import pallas as pl
from jax.experimental.pallas import tpu as pltpu
from jax.sharding import PartitionSpec as P

LOG2E = math.log2(math.e)
NEG = -1e30


def body(
    n_sp, n_tp, heads,
    q_ref, kv_ref, gate_ref, res_ref, wout_hbm, gain_ref, wup_hbm, wdn_hbm,
    out_ref,
    kv_all, gate_all, m_s, l_s, acc_s, att, att_in, wout, rsum,
    wu, wd, norm_all, hid, psend, pmate, pcomb, precv,
    kv_s1, kv_s2, kv_r, g_s1, g_s2, g_r, u_s1, u_s2, u_r, d_s1, d_s2, d_r,
    a_s, a_r, n_s, n_r, p_s, p_r, q_s, q_r, loc,
):
    ny = n_tp // 2
    nz = n_sp // ny
    tok, width = q_ref.shape
    hd = width // heads
    rows = tok // n_tp
    group = 2 * n_tp
    half = wu.shape[1]
    up_rows = wup_hbm.shape[0]
    features = res_ref.shape[1]
    cs = wdn_hbm.shape[1]
    me = lax.axis_index("sp")
    tp = lax.axis_index("tp")
    z, y = me // ny, me % ny
    par = z % 2
    slot = par * n_tp + tp

    def rcopy(src, dst, ss, rs, sp_to, tp_to=None):
        where = {"sp": sp_to} if tp_to is None else {"sp": sp_to, "tp": tp_to}
        return pltpu.make_async_remote_copy(
            src_ref=src, dst_ref=dst, send_sem=ss, recv_sem=rs,
            device_id=where, device_id_type=pl.DeviceIdType.MESH,
        )

    def member(o):
        other = (slot + o) % group
        return other, (z - par + other // n_tp) * ny + y, other % n_tp

    barrier = pltpu.get_barrier_semaphore()
    for dz in range(1, nz):
        pl.semaphore_signal(barrier, inc=1, device_id={"sp": ((z + dz) % nz) * ny + y},
                            device_id_type=pl.DeviceIdType.MESH)
    for dy in range(1, ny):
        pl.semaphore_signal(barrier, inc=1, device_id={"sp": z * ny + (y + dy) % ny},
                            device_id_type=pl.DeviceIdType.MESH)
    for o in range(1, group):
        _, sp_to, tp_to = member(o)
        pl.semaphore_signal(barrier, inc=1, device_id={"sp": sp_to, "tp": tp_to},
                            device_id_type=pl.DeviceIdType.MESH)
    pl.semaphore_wait(barrier, nz - 1 + ny - 1 + group - 1)

    def kv_up(zs):
        s = zs * ny + y
        to = me + ny
        return (rcopy(kv_all.at[s], kv_all.at[s], kv_s1.at[zs], kv_r.at[s], to),
                rcopy(gate_all.at[s], gate_all.at[s], g_s1.at[zs], g_r.at[s], to))

    def kv_first():
        to = me + ny
        return (rcopy(kv_ref, kv_all.at[me], kv_s1.at[z], kv_r.at[me], to),
                rcopy(gate_ref, gate_all.at[me], g_s1.at[z], g_r.at[me], to))

    def kv_own(dy):
        to = z * ny + (y + dy) % ny
        return (rcopy(kv_ref, kv_all.at[me], kv_s2.at[z * ny + dy], kv_r.at[me], to),
                rcopy(gate_ref, gate_all.at[me], g_s2.at[z * ny + dy], g_r.at[me], to))

    def kv_forward(zs, dy):
        s = zs * ny + y
        to = z * ny + (y + dy) % ny
        return (rcopy(kv_all.at[s], kv_all.at[s], kv_s2.at[zs * ny + dy], kv_r.at[s], to),
                rcopy(gate_all.at[s], gate_all.at[s], g_s2.at[zs * ny + dy], g_r.at[s], to))

    def wu_at(s):
        return wu.at[pl.ds(pl.multiple_of(s * up_rows, up_rows), up_rows), :]

    def up_half(p):
        return wup_hbm.at[:, pl.ds(pl.multiple_of(p * half, half), half)]

    def dn_half(p):
        return wdn_hbm.at[pl.ds(pl.multiple_of(p * half, half), half), :]

    def up_first(dz):
        zt = (z + dz) % nz
        return rcopy(up_half(zt % 2), wu_at(me), u_s1.at[dz], u_r.at[me], zt * ny + y)

    def dn_first(dz):
        zt = (z + dz) % nz
        return rcopy(dn_half(zt % 2), wd.at[me], d_s1.at[dz], d_r.at[me], zt * ny + y)

    def up_own(dy):
        return rcopy(up_half(par), wu_at(me), u_s2.at[z * ny + dy], u_r.at[me], z * ny + (y + dy) % ny)

    def dn_own(dy):
        return rcopy(dn_half(par), wd.at[me], d_s2.at[z * ny + dy], d_r.at[me], z * ny + (y + dy) % ny)

    def up_forward(zs, dy):
        s = zs * ny + y
        return rcopy(wu_at(s), wu_at(s), u_s2.at[zs * ny + dy], u_r.at[s], z * ny + (y + dy) % ny)

    def dn_forward(zs, dy):
        s = zs * ny + y
        return rcopy(wd.at[s], wd.at[s], d_s2.at[zs * ny + dy], d_r.at[s], z * ny + (y + dy) % ny)

    @pl.when(z + 1 < nz)
    def _():
        for c in kv_first():
            c.start()
    for dy in range(1, ny):
        @pl.when((y + dy) % ny > y)
        def _(dy=dy):
            for c in kv_own(dy):
                c.start()
    local_wout = pltpu.make_async_copy(wout_hbm, wout, loc.at[0])
    local_up = pltpu.make_async_copy(up_half(par), wu_at(me), loc.at[1])
    local_dn = pltpu.make_async_copy(dn_half(par), wd.at[me], loc.at[2])
    local_wout.start()
    local_up.start()
    local_dn.start()
    for dz in range(1, nz):
        @pl.when(z + dz >= nz)
        def _(dz=dz):
            up_first(dz).start()
    for dy in range(1, ny):
        up_own(dy).start()
    for dz in range(1, nz):
        @pl.when((z + dz >= nz) & (par == 0))
        def _(dz=dz):
            dn_first(dz).start()

    scale = hd ** (-0.5) * LOG2E

    def absorb(kv, gates, diagonal):
        for h in range(heads):
            cols = pl.ds(h * hd, hd)
            rel = (gates[h:h + 1, :] - gate_ref[h:h + 1, 0:1]) * LOG2E
            s = lax.dot_general(q_ref[:, cols], kv[:, cols], (((1,), (1,)), ((), ())),
                                preferred_element_type=jnp.float32)
            s = s * scale - rel
            if diagonal:
                qp = lax.broadcasted_iota(jnp.int32, s.shape, 0)
                kp = lax.broadcasted_iota(jnp.int32, s.shape, 1)
                s = jnp.where(kp <= qp, s, NEG)
            top = jnp.max(s, axis=1, keepdims=True)
            if not diagonal:
                old = m_s[:, h:h + 1]
                top = jnp.maximum(old, top)
                fade = jnp.exp2(old - top)
            w = jnp.exp2(s - top)
            total = jnp.sum(w, axis=1, keepdims=True)
            add = jnp.dot(w.astype(jnp.bfloat16), kv[:, pl.ds(width + h * hd, hd)],
                          preferred_element_type=jnp.float32)
            if not diagonal:
                total = l_s[:, h:h + 1] * fade + total
                add = acc_s[:, cols] * fade + add
            m_s[:, h:h + 1] = top
            l_s[:, h:h + 1] = total
            acc_s[:, cols] = add

    absorb(kv_ref, gate_ref, True)

    def level(i, carry):
        zs = z - i

        @pl.when(zs >= 0)
        def _():
            @pl.when(i > 0)
            def _():
                own = zs * ny + y
                rcopy(kv_ref, kv_all.at[own], kv_s1.at[0], kv_r.at[own], me).wait_recv()
                rcopy(gate_ref, gate_all.at[own], g_s1.at[0], g_r.at[own], me).wait_recv()

                @pl.when(z + 1 < nz)
                def _():
                    for c in kv_up(zs):
                        c.start()
                for dy in range(1, ny):
                    for c in kv_forward(zs, dy):
                        c.start()

            @pl.when(zs == 0)
            def _():
                for dz in range(1, nz):
                    @pl.when(z + dz < nz)
                    def _(dz=dz):
                        up_first(dz).start()
                for dz in range(1, nz):
                    @pl.when((z + dz < nz) & (par == 1))
                    def _(dz=dz):
                        dn_first(dz).start()

            def column(dy, carry):
                s = zs * ny + (y + dy) % ny

                @pl.when(s < me)
                def _():
                    @pl.when(dy > 0)
                    def _():
                        rcopy(kv_ref, kv_all.at[s], kv_s1.at[0], kv_r.at[s], me).wait_recv()
                        rcopy(gate_ref, gate_all.at[s], g_s1.at[0], g_r.at[s], me).wait_recv()
                    absorb(kv_all.at[s], gate_all.at[s], False)
                return carry

            lax.fori_loop(0, ny, column, 0)
        return carry

    lax.fori_loop(0, nz, level, 0)

    for h in range(heads):
        cols = pl.ds(h * hd, hd)
        done = (acc_s[:, cols] / l_s[:, h:h + 1]).astype(jnp.bfloat16)
        for j in range(n_tp):
            att[j, :, cols] = done[j * rows:(j + 1) * rows, :]

    def heads_to(o):
        to = (tp + o) % n_tp
        return rcopy(att.at[to], att_in.at[tp], a_s.at[o], a_r.at[tp], me, to)

    for o in range(1, n_tp):
        heads_to(o).start()
    for dz in range(1, nz):
        zs = (z - dz + nz) % nz
        s = zs * ny + y
        rcopy(up_half(0), wu_at(s), u_s1.at[0], u_r.at[s], me).wait_recv()
        for dy in range(1, ny):
            up_forward(zs, dy).start()
    for dy in range(1, ny):
        dn_own(dy).start()

    att_in[pl.ds(tp, 1)] = att[pl.ds(tp, 1)]
    local_wout.wait()
    for o in range(1, n_tp):
        src = (tp + o) % n_tp
        rcopy(att.at[0], att_in.at[src], a_s.at[0], a_r.at[src], me, tp).wait_recv()
    total = res_ref[...].astype(jnp.float32)
    for j in range(n_tp):
        total += jnp.dot(att_in[j], wout[j * width:(j + 1) * width, :], preferred_element_type=jnp.float32)
    rsum[...] = total
    mean_square = jnp.mean(total * total, axis=-1, keepdims=True)
    normed = (total * lax.rsqrt(mean_square + 1e-06) * gain_ref[...]).astype(jnp.bfloat16)

    chips = group // 2
    core = tp % 2
    mate = slot + 1 - 2 * core

    def block(ref, b):
        at = (b % 2) * chips + b // 2
        return ref.at[pl.ds(pl.multiple_of(at * rows, rows), rows), :]

    block(norm_all, slot)[...] = normed

    def normed_row(src, sem, other):
        zo, to = other // n_tp, other % n_tp
        return rcopy(block(norm_all, src), block(norm_all, src), n_s.at[sem], n_r.at[src],
                     (z - par + zo) * ny + y, to)

    def normed_chip(k):
        return normed_row(slot, k, (slot + 2 * k) % group)

    def normed_mate(k):
        return normed_row((slot + 2 * k) % group, chips + k, mate)

    for k in range(1, chips):
        normed_chip(k).start()
    normed_mate(0).start()
    for dz in range(1, nz):
        @pl.when((z + dz < nz) == (par == 0))
        def _(dz=dz):
            dn_first(dz).start()

    for k in range(1, chips):
        src = (slot + 2 * k) % group
        rcopy(block(norm_all, src), block(norm_all, src), n_s.at[0], n_r.at[src], me).wait_recv()
        normed_mate(k).start()

    def down_on(dz):
        zs = (z - dz + nz) % nz
        s = zs * ny + y
        rcopy(dn_half(0), wd.at[s], d_s1.at[0], d_r.at[s], me).wait_recv()
        for dy in range(1, ny):
            dn_forward(zs, dy).start()

    local_up.wait()
    for dy in range(1, ny):
        for zs in range(nz):
            s = zs * ny + (y + dy) % ny
            rcopy(up_half(0), wu_at(s), u_s1.at[0], u_r.at[s], me).wait_recv()
    for k in range(chips):
        src = (mate + 2 * k) % group
        rcopy(block(norm_all, src), block(norm_all, src), n_s.at[0], n_r.at[src], me).wait_recv()

    tile = min(256, half)

    def up_tile(i, carry):
        cols = pl.ds(pl.multiple_of(i * tile, tile), tile)
        u = jnp.maximum(jnp.dot(norm_all[...], wu[:, cols], preferred_element_type=jnp.float32), 0.0)
        hid[:, cols] = (u * u).astype(jnp.bfloat16)
        return carry

    lax.fori_loop(0, half // tile, up_tile, 0)

    per = max(1, 128 // cs)
    span = ny * cs

    mine = slot // 2

    def part(ref, at, count, zs):
        return ref.at[pl.ds(pl.multiple_of(at * rows, rows), count * rows),
                      pl.ds(pl.multiple_of(zs * span, span), span)]

    def to_mate(zs):
        return rcopy(part(psend, (1 - core) * chips, chips, zs), part(pmate, 0, chips, zs),
                     q_s.at[zs], q_r.at[zs], me, mate % n_tp)

    def partial_to(k, zs):
        chip = (mine + k) % chips
        other = chip * 2 + core
        return rcopy(part(pcomb, chip, 1, zs), part(precv, mine, 1, zs), p_s.at[k * nz + zs],
                     p_r.at[mine * nz + zs], (z - par + other // n_tp) * ny + y, other % n_tp)

    def level_of(dz):
        return (z - dz + nz) % nz

    def down_level(dz):
        zs = level_of(dz)
        for k in range(ny // per):
            ws = [wd[zs * ny + k * per + i] for i in range(per)]
            w = ws[0] if per == 1 else jnp.concatenate(ws, axis=1)
            cols = pl.ds(pl.multiple_of((zs * ny + k * per) * cs, per * cs), per * cs)
            psend[:, cols] = jnp.dot(hid[...], w, preferred_element_type=jnp.float32).astype(jnp.bfloat16)
        to_mate(zs).start()

    def combine(dz):
        zs = level_of(dz)
        to_mate(zs).wait_recv()
        both = (part(psend, core * chips, chips, zs)[...].astype(jnp.float32)
                + part(pmate, 0, chips, zs)[...].astype(jnp.float32))
        part(pcomb, 0, chips, zs)[...] = both.astype(jnp.bfloat16)
        for k in range(1, chips):
            partial_to(k, zs).start()

    local_dn.wait()
    for dz in range(nz):
        if dz + 1 < nz:
            down_on(dz + 1)
        zs = (z - dz + nz) % nz
        for dy in range(1, ny):
            s = zs * ny + (y + dy) % ny
            rcopy(dn_half(0), wd.at[s], d_s1.at[0], d_r.at[s], me).wait_recv()
        down_level(dz)
        if dz > 0:
            combine(dz - 1)
    combine(nz - 1)

    total = rsum[...]
    whole_row = lambda ref, at: ref[pl.ds(pl.multiple_of(at * rows, rows), rows), :].astype(jnp.float32)
    total += whole_row(pcomb, mine)
    for k in range(1, chips):
        src = (mine + k) % chips
        for zs in range(nz):
            rcopy(part(pcomb, src, 1, zs), part(precv, src, 1, zs), p_s.at[0], p_r.at[src * nz + zs], me).wait_recv()
        total += whole_row(precv, src)
    out_ref[...] = total.astype(jnp.bfloat16)

    @pl.when(z + 1 < nz)
    def _():
        for c in kv_first():
            c.wait_send()
    for dz in range(1, nz):
        @pl.when((z + 1 < nz) & (z - dz >= 0))
        def _(dz=dz):
            for c in kv_up(z - dz):
                c.wait_send()
        up_first(dz).wait_send()
        dn_first(dz).wait_send()
    for dy in range(1, ny):
        @pl.when((y + dy) % ny > y)
        def _(dy=dy):
            for c in kv_own(dy):
                c.wait_send()
        up_own(dy).wait_send()
        dn_own(dy).wait_send()
        for dz in range(1, nz):
            zs = (z - dz + nz) % nz

            @pl.when(z - dz >= 0)
            def _(zs=zs, dy=dy):
                for c in kv_forward(zs, dy):
                    c.wait_send()
            up_forward(zs, dy).wait_send()
            dn_forward(zs, dy).wait_send()
    for o in range(1, n_tp):
        heads_to(o).wait_send()
    for k in range(1, chips):
        normed_chip(k).wait_send()
    for k in range(chips):
        normed_mate(k).wait_send()
    for zs in range(nz):
        to_mate(zs).wait_send()
        for k in range(1, chips):
            partial_to(k, zs).wait_send()


def per_device(n_sp, n_tp, queries, keys, values, cum_gate, residual, w_out, gain, w_up, w_down):
    tok, width = queries.shape
    heads = cum_gate.shape[1]
    rows, features = residual.shape
    ny = n_tp // 2
    nz = n_sp // ny
    group = 2 * n_tp
    half = w_up.shape[1] // 2
    bf, f32 = jnp.bfloat16, jnp.float32
    gates = jnp.pad(cum_gate.T, ((0, 8 - heads), (0, 0)))
    kv = jnp.concatenate([keys, values], axis=1)
    vmem = pl.BlockSpec(memory_space=pltpu.VMEM)
    hbm = pl.BlockSpec(memory_space=pl.ANY)
    dma = lambda n: pltpu.SemaphoreType.DMA((n,))
    return pl.pallas_call(
        functools.partial(body, n_sp, n_tp, heads),
        out_shape=jax.ShapeDtypeStruct((rows, features), bf),
        in_specs=[vmem, vmem, vmem, vmem, hbm, vmem, hbm, hbm],
        out_specs=vmem,
        scratch_shapes=[
            pltpu.VMEM((n_sp, tok, 2 * width), bf),
            pltpu.VMEM((n_sp,) + gates.shape, f32),
            pltpu.VMEM((tok, 128), f32),
            pltpu.VMEM((tok, 128), f32),
            pltpu.VMEM((tok, width), f32),
            pltpu.VMEM((n_tp, rows, width), bf),
            pltpu.VMEM((n_tp, rows, width), bf),
            pltpu.VMEM(w_out.shape, bf),
            pltpu.VMEM((rows, features), f32),
            pltpu.VMEM((n_sp * w_up.shape[0], half), bf),
            pltpu.VMEM((n_sp, half, w_down.shape[1]), bf),
            pltpu.VMEM((group * rows, features), bf),
            pltpu.VMEM((group * rows, half), bf),
            pltpu.VMEM((group * rows, features), bf),
            pltpu.VMEM((n_tp * rows, features), bf),
            pltpu.VMEM((n_tp * rows, features), bf),
            pltpu.VMEM((n_tp * rows, features), bf),
        ]
        + [dma(nz), dma(n_sp), dma(n_sp)] * 4
        + [dma(n_tp), dma(n_tp), dma(group), dma(group), dma(group * nz), dma(group * nz), dma(nz), dma(nz), dma(3)],
        compiler_params=pltpu.CompilerParams(
            collective_id=0, has_side_effects=True, vmem_limit_bytes=63 * 1024 * 1024
        ),
    )(queries, kv, gates, residual, w_out, gain.reshape(1, -1), w_up, w_down)


def solution(mesh):
    n_sp, n_tp = mesh.shape["sp"], mesh.shape["tp"]
    return jax.shard_map(
        functools.partial(per_device, n_sp, n_tp),
        mesh=mesh,
        in_specs=(
            P("sp", "tp"),
            P("sp", "tp"),
            P("sp", "tp"),
            P("sp", "tp"),
            P(("sp", "tp"), None),
            P(),
            P(),
            P("sp", "tp"),
            P("tp", "sp"),
        ),
        out_specs=P(("sp", "tp"), None),
        check_vma=False,
    )
```

profile of v0, /device:TPU:19, one launch (start us, length us, event | category | flops | bytes accessed | tf_op | source)
XLA Modules:
  0.0 199.3 jit_solution(15531628317503406597)
XLA Ops:
  0.0 1.3 pad.4.gate_ref
  1.3 1.9 pad_maximum_fusion.kv_ref
  3.1 194.2 %shard_map.91 = bf16[128,2048]{1,0:T(8,128)(2,1)} custom-call(bf16[512,256]{1,0:T(8,128)(2,1)} %q_ref.1, bf16[512,512]{1,0:T(8,128)(2,1)} %pad_maximum_fusion.kv_ref, f32[8,512]{1,0:T(8,128)} %pad.4.gate_ref, bf16[128,2048]{1,0:T(8,128)(2,1)} %res_ref.1, bf16[1024,2048]{1,0:T(8,128)(2,1)} %wout_hbm.1, f32[1,2048]{1,0:T(1,128)} %bitcast.2, ...), custom_call_target="tpu_custom_call" | custom-call | tf_op jit(solution)/shard_map/pallas_call | solution.py:430
  197.4 1.9 copy.11
where the time goes:
time: 199 us
  Pallas kernels  194 us (97%)
  local copies, waits for them, and re-layouts  3.17 us (2%)
    pallas_call x1, Pallas kernels, per_device(): pl.pallas_call(functools.partial(body, n_sp, n_tp, heads), out_shape=jax....  194 us

commit v1 on v0

v1 whole, which is shorter than its diff:
```python
import functools
import math

import jax
import jax.numpy as jnp
from jax import lax
from jax.experimental import pallas as pl
from jax.experimental.pallas import tpu as pltpu
from jax.sharding import PartitionSpec as P

LOG2E = math.log2(math.e)
NEG = -1e30
STAT = 8


class Weights:
    def __init__(self, geo, rcopy, own, at, s_z, s_l, s_y, r):
        self.geo, self.rcopy, self.own, self.at = geo, rcopy, own, at
        self.s_z, self.s_l, self.s_y, self.r = s_z, s_l, s_y, r

    def mate(self, j):
        g = self.geo
        return g.par * g.hz + (g.zi + j) % g.hz

    def far(self, j):
        g = self.geo
        return (1 - g.par) * g.hz + (g.zi + j) % g.hz

    def to_mate(self, j):
        g = self.geo
        z = self.mate(j)
        return self.rcopy(self.own(g.par), self.at(g.me), self.s_z.at[j], self.r.at[g.me], z * g.ny + g.y)

    def to_partner(self):
        g = self.geo
        return self.rcopy(self.own(1 - g.par), self.at(g.me), self.s_z.at[0], self.r.at[g.me], self.far(0) * g.ny + g.y)

    def own_y(self, dy):
        g = self.geo
        return self.rcopy(self.own(g.par), self.at(g.me), self.s_y.at[g.z * g.ny + dy], self.r.at[g.me],
                          g.z * g.ny + (g.y + dy) % g.ny)

    def relay(self, j):
        g = self.geo
        s = self.far(0) * g.ny + g.y
        return self.rcopy(self.at(s), self.at(s), self.s_l.at[j], self.r.at[s], self.mate(j) * g.ny + g.y)

    def forward(self, zs, dy):
        g = self.geo
        s = zs * g.ny + g.y
        return self.rcopy(self.at(s), self.at(s), self.s_y.at[zs * g.ny + dy], self.r.at[s],
                          g.z * g.ny + (g.y + dy) % g.ny)

    def wait(self, s):
        self.rcopy(self.own(0), self.at(s), self.s_z.at[0], self.r.at[s], self.geo.me).wait_recv()

    def order(self, i):
        g = self.geo
        if i == 0:
            return g.z
        if i == 1:
            return self.far(0)
        return self.mate(i - 1) if i <= g.hz else self.far(i - g.hz)

    def service(self, i):
        g = self.geo
        zs = self.order(i)
        self.wait(zs * g.ny + g.y)
        if i == 1:
            for j in range(1, g.hz):
                self.relay(j).start()
        for dy in range(1, g.ny):
            self.forward(zs, dy).start()

    def level_wait(self, i):
        g = self.geo
        zs = self.order(i)
        for dy in range(1, g.ny):
            self.wait(zs * g.ny + (g.y + dy) % g.ny)

    def drain(self):
        g = self.geo
        for j in range(1, g.hz):
            self.to_mate(j).wait_send()
            self.relay(j).wait_send()
        self.to_partner().wait_send()
        for dy in range(1, g.ny):
            self.own_y(dy).wait_send()
            for i in range(1, g.nz):
                self.forward(self.order(i), dy).wait_send()


class Geo:
    pass


def body(
    n_sp, n_tp, heads,
    q_ref, k_ref, v_ref, gate_ref, res_ref, wout_hbm, gain_ref, wup_hbm, wdn_hbm,
    out_ref,
    q_all, k_all, v_all, g_all, o_send, o_recv, t_send, t_recv, st_s, m_s, l_s, acc_s,
    att, att_in, wout, rsum, wu, wd, norm_all, hid, psend, pmate, pcomb, precv,
    q_s, q_r, k_s, k_r, v_s, v_r, g_s, g_r, o_s, o_r, t_s, t_r,
    u_z, u_l, u_y, u_r, d_z, d_l, d_y, d_r,
    a_s, a_r, n_s, n_r, p_s, p_r, x_s, x_r, loc,
):
    ny = n_tp // 2
    nz = n_sp // ny
    hz = nz // 2
    cx = n_tp // 2
    tok, width = q_ref.shape
    hd = width // heads
    rows = tok // n_tp
    group = 2 * n_tp
    half = wu.shape[1]
    up_rows = wup_hbm.shape[0]
    cs = wdn_hbm.shape[1]
    me = lax.axis_index("sp")
    tp = lax.axis_index("tp")
    z, y = me // ny, me % ny
    par, zi = z // hz, z % hz
    x, core = tp // 2, tp % 2
    slot = par * n_tp + tp
    chips = group // 2
    mine = slot // 2
    mate = slot + 1 - 2 * core

    def rcopy(src, dst, ss, rs, sp_to, tp_to=None):
        where = {"sp": sp_to} if tp_to is None else {"sp": sp_to, "tp": tp_to}
        return pltpu.make_async_remote_copy(
            src_ref=src, dst_ref=dst, send_sem=ss, recv_sem=rs,
            device_id=where, device_id_type=pl.DeviceIdType.MESH,
        )

    def place(other):
        return ((other // n_tp) * hz + zi) * ny + y, other % n_tp

    k_all[pl.ds(y, 1)] = k_ref[...][None]
    v_all[pl.ds(y, 1)] = v_ref[...][None]
    g_all[pl.ds(y, 1)] = gate_ref[...][None]
    st_s[...] = jnp.zeros_like(st_s)
    t_recv[...] = jnp.zeros_like(t_recv)

    barrier = pltpu.get_barrier_semaphore()
    for dz in range(1, nz):
        pl.semaphore_signal(barrier, inc=1, device_id={"sp": ((z + dz) % nz) * ny + y},
                            device_id_type=pl.DeviceIdType.MESH)
    for dy in range(1, ny):
        pl.semaphore_signal(barrier, inc=1, device_id={"sp": z * ny + (y + dy) % ny},
                            device_id_type=pl.DeviceIdType.MESH)
    for o in range(1, group):
        sp_to, tp_to = place((slot + o) % group)
        pl.semaphore_signal(barrier, inc=1, device_id={"sp": sp_to, "tp": tp_to},
                            device_id_type=pl.DeviceIdType.MESH)
    with jax.named_scope("bar"):
        pl.semaphore_wait(barrier, nz - 1 + ny - 1 + group - 1)

    geo = Geo()
    geo.nz, geo.ny, geo.hz, geo.me, geo.z, geo.y, geo.par, geo.zi = nz, ny, hz, me, z, y, par, zi
    up = Weights(
        geo, rcopy,
        lambda p: wup_hbm.at[:, pl.ds(pl.multiple_of(p * half, half), half)],
        lambda s: wu.at[pl.ds(pl.multiple_of(s * up_rows, up_rows), up_rows), :],
        u_z, u_l, u_y, u_r,
    )
    dn = Weights(
        geo, rcopy,
        lambda p: wdn_hbm.at[pl.ds(pl.multiple_of(p * half, half), half), :],
        lambda s: wd.at[s],
        d_z, d_l, d_y, d_r,
    )

    def keys_to(dy):
        to = z * ny + (y + dy) % ny
        return (rcopy(k_ref, k_all.at[y], k_s.at[dy], k_r.at[y], to),
                rcopy(gate_ref, g_all.at[y], g_s.at[dy], g_r.at[y], to),
                rcopy(v_ref, v_all.at[y], v_s.at[dy], v_r.at[y], to))

    def keys_wanted(dy):
        return (z + 1 < nz) | ((y + dy) % ny > y)

    def query_to(zk):
        return rcopy(q_ref, q_all.at[z], q_s.at[zk], q_r.at[z], zk * ny + y)

    def part_to(zq):
        to = zq * ny + y
        at = pl.ds(pl.multiple_of(z * STAT, STAT), STAT)
        return (rcopy(o_send.at[zq], o_recv.at[z], o_s.at[zq], o_r.at[z], to),
                rcopy(t_send.at[zq], t_recv.at[at, :], t_s.at[zq], t_r.at[z], to))

    for dy in range(1, ny):
        @pl.when(keys_wanted(dy))
        def _(dy=dy):
            for c in keys_to(dy):
                c.start()
    for zk in range(nz - 1):
        @pl.when(zk < z)
        def _(zk=zk):
            query_to(zk).start()
    local_wout = pltpu.make_async_copy(wout_hbm, wout, loc.at[0])
    local_up = pltpu.make_async_copy(up.own(par), up.at(me), loc.at[1])
    local_dn = pltpu.make_async_copy(dn.own(par), dn.at(me), loc.at[2])
    local_up.start()
    local_dn.start()
    local_wout.start()
    up.to_partner().start()
    for j in range(1, hz):
        up.to_mate(j).start()
    for dy in range(1, ny):
        up.own_y(dy).start()
    for dy in range(1, ny):
        dn.own_y(dy).start()

    scale = hd ** (-0.5) * LOG2E

    def absorb(k, v, gates, diagonal):
        for h in range(heads):
            cols = pl.ds(h * hd, hd)
            rel = (gates[h:h + 1, :] - gate_ref[h:h + 1, 0:1]) * LOG2E
            s = lax.dot_general(q_ref[:, cols], k[:, cols], (((1,), (1,)), ((), ())),
                                preferred_element_type=jnp.float32)
            s = s * scale - rel
            if diagonal:
                qp = lax.broadcasted_iota(jnp.int32, s.shape, 0)
                kp = lax.broadcasted_iota(jnp.int32, s.shape, 1)
                s = jnp.where(kp <= qp, s, NEG)
            top = jnp.max(s, axis=1, keepdims=True)
            if not diagonal:
                old = m_s[:, h:h + 1]
                top = jnp.maximum(old, top)
                fade = jnp.exp2(old - top)
            w = jnp.exp2(s - top)
            total = jnp.sum(w, axis=1, keepdims=True)
            add = jnp.dot(w.astype(jnp.bfloat16), v[:, cols], preferred_element_type=jnp.float32)
            if not diagonal:
                total = l_s[:, h:h + 1] * fade + total
                add = acc_s[:, cols] * fade + add
            m_s[:, h:h + 1] = top
            l_s[:, h:h + 1] = total
            acc_s[:, cols] = add

    def partial(zq):
        for h in range(heads):
            cols = pl.ds(h * hd, hd)
            base = gate_ref[h:h + 1, 0:1] * LOG2E
            ss = []
            for i in range(ny):
                rel = g_all[i, h:h + 1, :] * LOG2E - base
                s = lax.dot_general(q_all[zq, :, cols], k_all[i, :, cols], (((1,), (1,)), ((), ())),
                                    preferred_element_type=jnp.float32)
                ss.append(s * scale - rel)
            top = jnp.max(functools.reduce(jnp.maximum, ss), axis=1, keepdims=True)
            total, add = 0.0, 0.0
            for i in range(ny):
                w = jnp.exp2(ss[i] - top)
                total += jnp.sum(w, axis=1, keepdims=True)
                add += jnp.dot(w.astype(jnp.bfloat16), v_all[i, :, cols], preferred_element_type=jnp.float32)
            o_send[zq, :, cols] = add.astype(jnp.bfloat16)
            st_s[:, h:h + 1] = top - base
            st_s[:, heads + h:heads + h + 1] = total
        t_send[zq] = jnp.transpose(st_s[...])[0:STAT, :]

    with jax.named_scope("diag"):
        absorb(k_ref, v_ref, gate_ref, True)

    for dy in range(1, ny):
        src = (y + dy) % ny

        @pl.when((z + 1 < nz) | (src < y))
        def _(dy=dy, src=src):
            with jax.named_scope("kvwait"):
                for ref, all_, ss, rs in ((k_ref, k_all, k_s, k_r), (gate_ref, g_all, g_s, g_r), (v_ref, v_all, v_s, v_r)):
                    rcopy(ref, all_.at[src], ss.at[0], rs.at[src], me).wait_recv()

            @pl.when(src < y)
            def _():
                with jax.named_scope("absorb"):
                    absorb(k_all.at[src], v_all.at[src], g_all.at[src], False)

    def query_level(i, carry):
        zq = nz - 1 - i

        @pl.when(zq > z)
        def _():
            with jax.named_scope("qwait"):
                rcopy(q_ref, q_all.at[zq], q_s.at[0], q_r.at[zq], me).wait_recv()
            with jax.named_scope("partial"):
                partial(zq)
            for c in part_to(zq):
                c.start()
        return carry

    lax.fori_loop(0, nz, query_level, 0)

    with jax.named_scope("upsvc"):
        for i in range(1, hz + 1):
            up.service(i)

    for zk in range(nz - 1):
        @pl.when(zk < z)
        def _(zk=zk):
            with jax.named_scope("owait"):
                at = pl.ds(zk * STAT, STAT)
                rcopy(o_send.at[0], o_recv.at[zk], o_s.at[0], o_r.at[zk], me).wait_recv()
                rcopy(t_send.at[0], t_recv.at[at, :], t_s.at[0], t_r.at[zk], me).wait_recv()

    @pl.when(z > 0)
    def _():
        st_s[...] = jnp.transpose(t_recv[...])

    for zk in range(nz - 1):
        @pl.when(zk < z)
        def _(zk=zk):
            for h in range(heads):
                cols = pl.ds(h * hd, hd)
                at = zk * STAT + h
                their = st_s[:, at:at + 1] + gate_ref[h:h + 1, 0:1] * LOG2E
                old = m_s[:, h:h + 1]
                top = jnp.maximum(old, their)
                fade, rise = jnp.exp2(old - top), jnp.exp2(their - top)
                m_s[:, h:h + 1] = top
                l_s[:, h:h + 1] = l_s[:, h:h + 1] * fade + st_s[:, at + heads:at + heads + 1] * rise
                acc_s[:, cols] = acc_s[:, cols] * fade + o_recv[zk, :, cols].astype(jnp.float32) * rise

    for h in range(heads):
        cols = pl.ds(h * hd, hd)
        done = (acc_s[:, cols] / l_s[:, h:h + 1]).astype(jnp.bfloat16)
        for j in range(n_tp):
            att[j, :, cols] = done[j * rows:(j + 1) * rows, :]

    def heads_to(o):
        to = (tp + o) % n_tp
        return rcopy(att.at[to], att_in.at[tp], a_s.at[o], a_r.at[tp], me, to)

    for o in range(1, n_tp):
        heads_to(o).start()
    att_in[pl.ds(tp, 1)] = att[pl.ds(tp, 1)]
    local_wout.wait()
    with jax.named_scope("attwait"):
        for o in range(1, n_tp):
            src = (tp + o) % n_tp
            rcopy(att.at[0], att_in.at[src], a_s.at[0], a_r.at[src], me, tp).wait_recv()
    total = res_ref[...].astype(jnp.float32)
    for j in range(n_tp):
        total += jnp.dot(att_in[j], wout[j * width:(j + 1) * width, :], preferred_element_type=jnp.float32)
    rsum[...] = total
    mean_square = jnp.mean(total * total, axis=-1, keepdims=True)
    normed = (total * lax.rsqrt(mean_square + 1e-06) * gain_ref[...]).astype(jnp.bfloat16)

    def block(ref, b):
        at = (b % 2) * chips + b // 2
        return ref.at[pl.ds(pl.multiple_of(at * rows, rows), rows), :]

    block(norm_all, slot)[...] = normed

    def normed_row(src, sem, other):
        sp_to, tp_to = place(other)
        return rcopy(block(norm_all, src), block(norm_all, src), n_s.at[sem], n_r.at[src], sp_to, tp_to)

    def beside(k):
        return par * n_tp + ((x + k) % cx) * 2 + core

    across = (1 - par) * n_tp + tp

    def normed_beside(k):
        return normed_row(slot, k, beside(k))

    def normed_across():
        return normed_row(slot, 0, across)

    def normed_relay(k):
        return normed_row(across, cx + k, beside(k))

    def normed_mate(k):
        return normed_row((slot + 2 * k) % group, chips + k, mate)

    def normed_wait(src):
        rcopy(block(norm_all, src), block(norm_all, src), n_s.at[0], n_r.at[src], me).wait_recv()

    normed_across().start()
    for k in range(1, cx):
        normed_beside(k).start()
    normed_mate(0).start()

    dn.to_partner().start()
    for j in range(1, hz):
        dn.to_mate(j).start()

    with jax.named_scope("upsvc2"):
        for i in range(hz + 1, nz):
            up.service(i)

    with jax.named_scope("normwait_across"):
        normed_wait(across)
    for k in range(1, cx):
        normed_relay(k).start()
    with jax.named_scope("normwait_chip"):
        normed_mate(chips // 2).start()
        for k in range(1, chips):
            if k != chips // 2:
                normed_wait((slot + 2 * k) % group)
                normed_mate(k).start()

    local_up.wait()
    with jax.named_scope("upwait_y"):
        for i in range(nz):
            up.level_wait(i)
    with jax.named_scope("normwait_mate"):
        for k in range(chips):
            normed_wait((mate + 2 * k) % group)

    tile = min(256, half)

    def up_tile(i, carry):
        cols = pl.ds(pl.multiple_of(i * tile, tile), tile)
        u = jnp.maximum(jnp.dot(norm_all[...], wu[:, cols], preferred_element_type=jnp.float32), 0.0)
        hid[:, cols] = (u * u).astype(jnp.bfloat16)
        return carry

    with jax.named_scope("up_mm"):
        lax.fori_loop(0, half // tile, up_tile, 0)

    per = max(1, 128 // cs)
    span = ny * cs

    def part(ref, at, count, zs):
        return ref.at[pl.ds(pl.multiple_of(at * rows, rows), count * rows),
                      pl.ds(pl.multiple_of(zs * span, span), span)]

    def to_mate(zs):
        return rcopy(part(psend, (1 - core) * chips, chips, zs), part(pmate, 0, chips, zs),
                     x_s.at[zs], x_r.at[zs], me, mate % n_tp)

    def partial_to(k, zs):
        chip = (mine + k) % chips
        sp_to, tp_to = place(chip * 2 + core)
        return rcopy(part(pcomb, chip, 1, zs), part(precv, mine, 1, zs), p_s.at[k * nz + zs],
                     p_r.at[mine * nz + zs], sp_to, tp_to)

    def down_level(zs):
        for k in range(ny // per):
            ws = [wd[zs * ny + k * per + i] for i in range(per)]
            w = ws[0] if per == 1 else jnp.concatenate(ws, axis=1)
            cols = pl.ds(pl.multiple_of((zs * ny + k * per) * cs, per * cs), per * cs)
            psend[:, cols] = jnp.dot(hid[...], w, preferred_element_type=jnp.float32).astype(jnp.bfloat16)
        to_mate(zs).start()

    def combine(zs):
        with jax.named_scope("matewait"):
            to_mate(zs).wait_recv()
        both = (part(psend, core * chips, chips, zs)[...].astype(jnp.float32)
                + part(pmate, 0, chips, zs)[...].astype(jnp.float32))
        part(pcomb, 0, chips, zs)[...] = both.astype(jnp.bfloat16)
        for k in range(1, chips):
            partial_to(k, zs).start()

    local_dn.wait()
    for i in range(nz):
        if i + 1 < nz:
            with jax.named_scope("dnwait_z"):
                dn.service(i + 1)
        with jax.named_scope("dnwait_y"):
            dn.level_wait(i)
        with jax.named_scope("down_mm"):
            down_level(dn.order(i))
        if i > 0:
            combine(dn.order(i - 1))
    combine(dn.order(nz - 1))

    total = rsum[...]
    whole_row = lambda ref, at: ref[pl.ds(pl.multiple_of(at * rows, rows), rows), :].astype(jnp.float32)
    total += whole_row(pcomb, mine)
    for k in range(1, chips):
        src = (mine + k) % chips
        with jax.named_scope("partwait"):
            for zs in range(nz):
                rcopy(part(pcomb, src, 1, zs), part(precv, src, 1, zs), p_s.at[0], p_r.at[src * nz + zs], me).wait_recv()
        total += whole_row(precv, src)
    out_ref[...] = total.astype(jnp.bfloat16)

    for dy in range(1, ny):
        @pl.when(keys_wanted(dy))
        def _(dy=dy):
            for c in keys_to(dy):
                c.wait_send()
    for zk in range(nz - 1):
        @pl.when(zk < z)
        def _(zk=zk):
            query_to(zk).wait_send()
    for zq in range(1, nz):
        @pl.when(zq > z)
        def _(zq=zq):
            for c in part_to(zq):
                c.wait_send()
    up.drain()
    dn.drain()
    for o in range(1, n_tp):
        heads_to(o).wait_send()
    normed_across().wait_send()
    for k in range(1, cx):
        normed_beside(k).wait_send()
        normed_relay(k).wait_send()
    for k in range(chips):
        normed_mate(k).wait_send()
    for zs in range(nz):
        to_mate(zs).wait_send()
        for k in range(1, chips):
            partial_to(k, zs).wait_send()


def per_device(n_sp, n_tp, queries, keys, values, cum_gate, residual, w_out, gain, w_up, w_down):
    tok, width = queries.shape
    heads = cum_gate.shape[1]
    rows, features = residual.shape
    ny = n_tp // 2
    nz = n_sp // ny
    hz = nz // 2
    group = 2 * n_tp
    half = w_up.shape[1] // 2
    bf, f32 = jnp.bfloat16, jnp.float32
    assert nz % 2 == 0 and 2 * heads <= STAT
    gates = jnp.pad(cum_gate.T, ((0, 8 - heads), (0, 0)))
    vmem = pl.BlockSpec(memory_space=pltpu.VMEM)
    hbm = pl.BlockSpec(memory_space=pl.ANY)
    dma = lambda n: pltpu.SemaphoreType.DMA((n,))
    lanes = max(128, nz * STAT)
    return pl.pallas_call(
        functools.partial(body, n_sp, n_tp, heads),
        out_shape=jax.ShapeDtypeStruct((rows, features), bf),
        in_specs=[vmem, vmem, vmem, vmem, vmem, hbm, vmem, hbm, hbm],
        out_specs=vmem,
        scratch_shapes=[
            pltpu.VMEM((nz, tok, width), bf),
            pltpu.VMEM((ny, tok, width), bf),
            pltpu.VMEM((ny, tok, width), bf),
            pltpu.VMEM((ny,) + gates.shape, f32),
            pltpu.VMEM((nz, tok, width), bf),
            pltpu.VMEM((nz, tok, width), bf),
            pltpu.VMEM((nz, STAT, tok), f32),
            pltpu.VMEM((lanes, tok), f32),
            pltpu.VMEM((tok, lanes), f32),
            pltpu.VMEM((tok, 128), f32),
            pltpu.VMEM((tok, 128), f32),
            pltpu.VMEM((tok, width), f32),
            pltpu.VMEM((n_tp, rows, width), bf),
            pltpu.VMEM((n_tp, rows, width), bf),
            pltpu.VMEM(w_out.shape, bf),
            pltpu.VMEM((rows, features), f32),
            pltpu.VMEM((n_sp * w_up.shape[0], half), bf),
            pltpu.VMEM((n_sp, half, w_down.shape[1]), bf),
            pltpu.VMEM((group * rows, features), bf),
            pltpu.VMEM((group * rows, half), bf),
            pltpu.VMEM((group * rows, features), bf),
            pltpu.VMEM((n_tp * rows, features), bf),
            pltpu.VMEM((n_tp * rows, features), bf),
            pltpu.VMEM((n_tp * rows, features), bf),
        ]
        + [dma(nz), dma(nz)] + [dma(ny)] * 6 + [dma(nz)] * 4
        + [dma(hz), dma(hz), dma(n_sp), dma(n_sp)] * 2
        + [dma(n_tp), dma(n_tp), dma(group + n_tp), dma(group), dma(n_tp * nz), dma(n_tp * nz), dma(nz), dma(nz), dma(3)],
        compiler_params=pltpu.CompilerParams(
            collective_id=0, has_side_effects=True, vmem_limit_bytes=63 * 1024 * 1024
        ),
    )(queries, keys, values, gates, residual, w_out, gain.reshape(1, -1), w_up, w_down)


def solution(mesh):
    n_sp, n_tp = mesh.shape["sp"], mesh.shape["tp"]
    return jax.shard_map(
        functools.partial(per_device, n_sp, n_tp),
        mesh=mesh,
        in_specs=(
            P("sp", "tp"),
            P("sp", "tp"),
            P("sp", "tp"),
            P("sp", "tp"),
            P(("sp", "tp"), None),
            P(),
            P(),
            P("sp", "tp"),
            P("tp", "sp"),
        ),
        out_specs=P(("sp", "tp"), None),
        check_vma=False,
    )
```

time: 199 us -> 176 us (0.88)
  the two profiles are of different devices: /device:TPU:19 before, /device:TPU:0 now
where the time goes in v1:
time: 176 us; the launch traced here: 173 us
  Pallas kernels  170 us (97%)
  local copies, waits for them, and re-layouts  3.18 us (2%)
    pallas_call x1, Pallas kernels, per_device(): pl.pallas_call(functools.partial(body, n_sp, n_tp, heads), out_shape=jax....  170 us

profile of v1, /device:TPU:0, one launch (start us, length us, event | category | flops | bytes accessed | tf_op | source)
XLA Modules:
  0.0 172.7 jit_solution(5967654713105651137)
XLA Ops:
  0.0 1.3 pad.4.gate_ref
  1.3 169.5 %shard_map.91 = bf16[128,2048]{1,0:T(8,128)(2,1)} custom-call(bf16[512,256]{1,0:T(8,128)(2,1)} %q_ref.1, bf16[512,256]{1,0:T(8,128)(2,1)} %k_ref.1, bf16[512,256]{1,0:T(8,128)(2,1)} %v_ref.1, f32[8,512]{1,0:T(8,128)} %pad.4.gate_ref, bf16[128,2048]{1,0:T(8,128)(2,1)} %res_ref.1, bf16[1024,2048]{1,0:T(8,128)(2,1)} %wout_hbm.1, f32[1,2048]{1,0:T(1,128)} %bitcast.2, ...), custom_call_target="tpu_custom_call" | custom-call | tf_op jit(solution)/shard_map/pallas_call | solution.py:527
  170.8 1.9 %copy.11 = bf16[128,2048]{1,0:T(8,128)(2,1)} copy(bf16[128,2048]{1,0:T(8,128)(2,1)} %shard_map.91) | data formatting | bytes 1048576

commit v2 on v1

--- a/solution.py
+++ b/solution.py
@@ -11,11 +11,12 @@
 LOG2E = math.log2(math.e)
 NEG = -1e30
 STAT = 8
+CUTS = 2
 
 
 class Weights:
-    def __init__(self, geo, rcopy, own, at, s_z, s_l, s_y, r):
-        self.geo, self.rcopy, self.own, self.at = geo, rcopy, own, at
+    def __init__(self, geo, cuts, rcopy, own, at, s_z, s_l, s_y, r):
+        self.geo, self.cuts, self.rcopy, self.own, self.at = geo, cuts, rcopy, own, at
         self.s_z, self.s_l, self.s_y, self.r = s_z, s_l, s_y, r
 
     def mate(self, j):
@@ -26,68 +27,59 @@
         g = self.geo
         return (1 - g.par) * g.hz + (g.zi + j) % g.hz
 
-    def to_mate(self, j):
-        g = self.geo
-        z = self.mate(j)
-        return self.rcopy(self.own(g.par), self.at(g.me), self.s_z.at[j], self.r.at[g.me], z * g.ny + g.y)
-
-    def to_partner(self):
-        g = self.geo
-        return self.rcopy(self.own(1 - g.par), self.at(g.me), self.s_z.at[0], self.r.at[g.me], self.far(0) * g.ny + g.y)
-
-    def own_y(self, dy):
-        g = self.geo
-        return self.rcopy(self.own(g.par), self.at(g.me), self.s_y.at[g.z * g.ny + dy], self.r.at[g.me],
-                          g.z * g.ny + (g.y + dy) % g.ny)
-
-    def relay(self, j):
+    def send(self, src, s, c, sem, k, z, y):
+        return self.rcopy(src, self.at(s, c), sem.at[k * self.cuts + c], self.r.at[s * self.cuts + c], z * self.geo.ny + y)
+
+    def to_mate(self, j, c):
+        g = self.geo
+        return self.send(self.own(g.par, c), g.me, c, self.s_z, j, self.mate(j), g.y)
+
+    def to_partner(self, c):
+        g = self.geo
+        return self.send(self.own(1 - g.par, c), g.me, c, self.s_z, 0, self.far(0), g.y)
+
+    def own_y(self, dy, c):
+        g = self.geo
+        return self.send(self.own(g.par, c), g.me, c, self.s_y, g.z * g.ny + dy, g.z, (g.y + dy) % g.ny)
+
+    def relay(self, j, c):
         g = self.geo
         s = self.far(0) * g.ny + g.y
-        return self.rcopy(self.at(s), self.at(s), self.s_l.at[j], self.r.at[s], self.mate(j) * g.ny + g.y)
-
-    def forward(self, zs, dy):
+        return self.send(self.at(s, c), s, c, self.s_l, j, self.mate(j), g.y)
+
+    def forward(self, zs, dy, c):
         g = self.geo
         s = zs * g.ny + g.y
-        return self.rcopy(self.at(s), self.at(s), self.s_y.at[zs * g.ny + dy], self.r.at[s],
-                          g.z * g.ny + (g.y + dy) % g.ny)
-
-    def wait(self, s):
-        self.rcopy(self.own(0), self.at(s), self.s_z.at[0], self.r.at[s], self.geo.me).wait_recv()
+        return self.send(self.at(s, c), s, c, self.s_y, zs * g.ny + dy, g.z, (g.y + dy) % g.ny)
+
+    def wait(self, s, c):
+        self.rcopy(self.own(0, c), self.at(s, c), self.s_z.at[0], self.r.at[s * self.cuts + c], self.geo.me).wait_recv()
 
     def order(self, i):
         g = self.geo
-        if i == 0:
-            return g.z
-        if i == 1:
-            return self.far(0)
-        return self.mate(i - 1) if i <= g.hz else self.far(i - g.hz)
-
-    def service(self, i):
+        return self.mate(i) if i < g.hz else self.far(i - g.hz)
+
+    def service(self, i, c):
         g = self.geo
         zs = self.order(i)
-        self.wait(zs * g.ny + g.y)
-        if i == 1:
+        self.wait(zs * g.ny + g.y, c)
+        if i == g.hz:
             for j in range(1, g.hz):
-                self.relay(j).start()
+                self.relay(j, c).start()
         for dy in range(1, g.ny):
-            self.forward(zs, dy).start()
-
-    def level_wait(self, i):
-        g = self.geo
-        zs = self.order(i)
-        for dy in range(1, g.ny):
-            self.wait(zs * g.ny + (g.y + dy) % g.ny)
+            self.forward(zs, dy, c).start()
 
     def drain(self):
         g = self.geo
-        for j in range(1, g.hz):
-            self.to_mate(j).wait_send()
-            self.relay(j).wait_send()
-        self.to_partner().wait_send()
-        for dy in range(1, g.ny):
-            self.own_y(dy).wait_send()
-            for i in range(1, g.nz):
-                self.forward(self.order(i), dy).wait_send()
+        for c in range(self.cuts):
+            for j in range(1, g.hz):
+                self.to_mate(j, c).wait_send()
+                self.relay(j, c).wait_send()
+            self.to_partner(c).wait_send()
+            for dy in range(1, g.ny):
+                self.own_y(dy, c).wait_send()
+                for i in range(1, g.nz):
+                    self.forward(self.order(i), dy, c).wait_send()
 
 
 class Geo:
@@ -99,10 +91,10 @@
     q_ref, k_ref, v_ref, gate_ref, res_ref, wout_hbm, gain_ref, wup_hbm, wdn_hbm,
     out_ref,
     q_all, k_all, v_all, g_all, o_send, o_recv, t_send, t_recv, st_s, m_s, l_s, acc_s,
-    att, att_in, wout, rsum, wu, wd, norm_all, hid, psend, pmate, pcomb, precv,
+    att, att_in, wout, rsum, wu, wd, norm_all, hid, psend, pmate, pcomb, precv, pfar, pback,
     q_s, q_r, k_s, k_r, v_s, v_r, g_s, g_r, o_s, o_r, t_s, t_r,
     u_z, u_l, u_y, u_r, d_z, d_l, d_y, d_r,
-    a_s, a_r, n_s, n_r, p_s, p_r, x_s, x_r, loc,
+    a_s, a_r, n_s, n_r, p_s, p_r, x_s, x_r, f_s, f_r, loc,
 ):
     ny = n_tp // 2
     nz = n_sp // ny
@@ -157,16 +149,18 @@
 
     geo = Geo()
     geo.nz, geo.ny, geo.hz, geo.me, geo.z, geo.y, geo.par, geo.zi = nz, ny, hz, me, z, y, par, zi
+    cuts = CUTS
+    upc, dnc = up_rows // cuts, half // cuts
     up = Weights(
-        geo, rcopy,
-        lambda p: wup_hbm.at[:, pl.ds(pl.multiple_of(p * half, half), half)],
-        lambda s: wu.at[pl.ds(pl.multiple_of(s * up_rows, up_rows), up_rows), :],
+        geo, cuts, rcopy,
+        lambda p, c: wup_hbm.at[pl.ds(c * upc, upc), pl.ds(pl.multiple_of(p * half, half), half)],
+        lambda s, c: wu.at[pl.ds(pl.multiple_of(s * up_rows + c * upc, upc), upc), :],
         u_z, u_l, u_y, u_r,
     )
     dn = Weights(
-        geo, rcopy,
-        lambda p: wdn_hbm.at[pl.ds(pl.multiple_of(p * half, half), half), :],
-        lambda s: wd.at[s],
+        geo, cuts, rcopy,
+        lambda p, c: wdn_hbm.at[pl.ds(pl.multiple_of(p * half + c * dnc, dnc), dnc), :],
+        lambda s, c: wd.at[s, pl.ds(c * dnc, dnc), :],
         d_z, d_l, d_y, d_r,
     )
 
@@ -179,8 +173,14 @@
     def keys_wanted(dy):
         return (z + 1 < nz) | ((y + dy) % ny > y)
 
-    def query_to(zk):
-        return rcopy(q_ref, q_all.at[z], q_s.at[zk], q_r.at[z], zk * ny + y)
+    def query_first():
+        return rcopy(q_ref, q_all.at[z], q_s.at[z], q_r.at[z], me - ny)
+
+    def query_on(zq):
+        return rcopy(q_all.at[zq], q_all.at[zq], q_s.at[zq], q_r.at[zq], me - ny)
+
+    def query_wait(zq):
+        rcopy(q_ref, q_all.at[zq], q_s.at[0], q_r.at[zq], me).wait_recv()
 
     def part_to(zq):
         to = zq * ny + y
@@ -193,23 +193,39 @@
         def _(dy=dy):
             for c in keys_to(dy):
                 c.start()
-    for zk in range(nz - 1):
-        @pl.when(zk < z)
-        def _(zk=zk):
-            query_to(zk).start()
+    @pl.when(z > 0)
+    def _():
+        query_first().start()
     local_wout = pltpu.make_async_copy(wout_hbm, wout, loc.at[0])
-    local_up = pltpu.make_async_copy(up.own(par), up.at(me), loc.at[1])
-    local_dn = pltpu.make_async_copy(dn.own(par), dn.at(me), loc.at[2])
+    local_up = pltpu.make_async_copy(
+        wup_hbm.at[:, pl.ds(pl.multiple_of(par * half, half), half)],
+        wu.at[pl.ds(pl.multiple_of(me * up_rows, up_rows), up_rows), :], loc.at[1])
+    local_dn = pltpu.make_async_copy(
+        wdn_hbm.at[pl.ds(pl.multiple_of(par * half, half), half), :], wd.at[me], loc.at[2])
+
+    def direct_mates(w, upward):
+        for j in range(1, hz):
+            @pl.when((w.mate(j) > z) if upward else (w.mate(j) < z))
+            def _(j=j):
+                for c in range(cuts):
+                    w.to_mate(j, c).start()
+
+    def direct_partner(w, upward, chunks):
+        @pl.when(par == (0 if upward else 1))
+        def _():
+            for c in chunks:
+                w.to_partner(c).start()
+
+    every = range(cuts)
+    direct_partner(up, True, every)
+    direct_mates(up, True)
     local_up.start()
     local_dn.start()
     local_wout.start()
-    up.to_partner().start()
-    for j in range(1, hz):
-        up.to_mate(j).start()
-    for dy in range(1, ny):
-        up.own_y(dy).start()
-    for dy in range(1, ny):
-        dn.own_y(dy).start()
+    for w in (up, dn):
+        for dy in range(1, ny):
+            for c in every:
+                w.own_y(dy, c).start()
 
     scale = hd ** (-0.5) * LOG2E
 
@@ -263,6 +279,15 @@
     with jax.named_scope("diag"):
         absorb(k_ref, v_ref, gate_ref, True)
 
+    for zq in range(2, nz):
+        @pl.when((zq > z) & (z > 0))
+        def _(zq=zq):
+            with jax.named_scope("qfwd"):
+                query_wait(zq)
+            query_on(zq).start()
+    direct_mates(up, False)
+    direct_partner(up, False, every)
+
     for dy in range(1, ny):
         src = (y + dy) % ny
 
@@ -278,23 +303,32 @@
                     absorb(k_all.at[src], v_all.at[src], g_all.at[src], False)
 
     def query_level(i, carry):
-        zq = nz - 1 - i
+        zq = i + 1
 
         @pl.when(zq > z)
         def _():
-            with jax.named_scope("qwait"):
-                rcopy(q_ref, q_all.at[zq], q_s.at[0], q_r.at[zq], me).wait_recv()
+            @pl.when(z == 0)
+            def _():
+                with jax.named_scope("qwait"):
+                    query_wait(zq)
             with jax.named_scope("partial"):
                 partial(zq)
             for c in part_to(zq):
                 c.start()
         return carry
 
-    lax.fori_loop(0, nz, query_level, 0)
+    lax.fori_loop(0, nz - 1, query_level, 0)
 
     with jax.named_scope("upsvc"):
-        for i in range(1, hz + 1):
-            up.service(i)
+        for i in [hz] + list(range(1, hz)):
+            for c in every:
+                up.service(i, c)
+    direct_partner(dn, False, every)
+    direct_partner(dn, True, [0])
+    for p in range(2):
+        @pl.when(par == p)
+        def _(p=p):
+            direct_mates(dn, p == 1)
 
     for zk in range(nz - 1):
         @pl.when(zk < z)
@@ -352,62 +386,102 @@
         return ref.at[pl.ds(pl.multiple_of(at * rows, rows), rows), :]
 
     block(norm_all, slot)[...] = normed
-
-    def normed_row(src, sem, other):
+    strips = 2
+    strip = norm_all.shape[1] // strips
+
+    def strip_of(b, c):
+        at = (b % 2) * chips + b // 2
+        return norm_all.at[pl.ds(pl.multiple_of(at * rows, rows), rows), pl.ds(c * strip, strip)]
+
+    def normed_row(src, sem, other, c):
         sp_to, tp_to = place(other)
-        return rcopy(block(norm_all, src), block(norm_all, src), n_s.at[sem], n_r.at[src], sp_to, tp_to)
+        return rcopy(strip_of(src, c), strip_of(src, c), n_s.at[sem * strips + c], n_r.at[src * strips + c], sp_to, tp_to)
 
     def beside(k):
         return par * n_tp + ((x + k) % cx) * 2 + core
 
     across = (1 - par) * n_tp + tp
 
-    def normed_beside(k):
-        return normed_row(slot, k, beside(k))
-
-    def normed_across():
-        return normed_row(slot, 0, across)
-
-    def normed_relay(k):
-        return normed_row(across, cx + k, beside(k))
-
-    def normed_mate(k):
-        return normed_row((slot + 2 * k) % group, chips + k, mate)
-
-    def normed_wait(src):
-        rcopy(block(norm_all, src), block(norm_all, src), n_s.at[0], n_r.at[src], me).wait_recv()
-
-    normed_across().start()
-    for k in range(1, cx):
-        normed_beside(k).start()
-    normed_mate(0).start()
-
-    dn.to_partner().start()
-    for j in range(1, hz):
-        dn.to_mate(j).start()
+    def normed_beside(k, c):
+        return normed_row(slot, k, beside(k), c)
+
+    def normed_across(c):
+        return normed_row(slot, 0, across, c)
+
+    def normed_relay(k, c):
+        return normed_row(across, cx + k, beside(k), c)
+
+    def normed_mate(k, c):
+        return normed_row((slot + 2 * k) % group, chips + k, mate, c)
+
+    def normed_wait(src, c):
+        rcopy(strip_of(src, c), strip_of(src, c), n_s.at[0], n_r.at[src * strips + c], me).wait_recv()
+
+    for c in range(strips):
+        normed_across(c).start()
+    for c in range(strips):
+        for k in range(1, cx):
+            normed_beside(k, c).start()
+    for c in range(strips):
+        normed_mate(0, c).start()
+    direct_partner(dn, True, range(1, cuts))
+    for p in range(2):
+        @pl.when(par == p)
+        def _(p=p):
+            direct_mates(dn, p == 0)
 
     with jax.named_scope("upsvc2"):
         for i in range(hz + 1, nz):
-            up.service(i)
-
-    with jax.named_scope("normwait_across"):
-        normed_wait(across)
-    for k in range(1, cx):
-        normed_relay(k).start()
-    with jax.named_scope("normwait_chip"):
-        normed_mate(chips // 2).start()
-        for k in range(1, chips):
-            if k != chips // 2:
-                normed_wait((slot + 2 * k) % group)
-                normed_mate(k).start()
-
+            for c in every:
+                up.service(i, c)
+
+    def dn_service(i, chunks, name):
+        for c in chunks:
+            with jax.named_scope(name):
+                dn.service(i, c)
+
+    def dn_mates(soon):
+        for j in range(1, hz):
+            zs = dn.mate(j)
+
+            @pl.when((zs < z) == ((par == 1) == soon))
+            def _(j=j):
+                dn_service(j, every, "dnsvc_mate")
+
+    dn_service(hz, [0], "dnsvc_part0")
+
+    @pl.when(par == 0)
+    def _():
+        dn_service(hz, range(1, cuts), "dnsvc_part1")
+    dn_mates(True)
+
+    for c in range(strips):
+        with jax.named_scope("normwait_across"):
+            normed_wait(across, c)
+        for k in range(1, cx):
+            normed_relay(k, c).start()
+        normed_mate(chips // 2, c).start()
+    for near in (True, False):
+        for k in range(1, cx):
+            for c in range(strips):
+                b = beside(k) if near else (1 - par) * n_tp + ((x + k) % cx) * 2 + core
+                with jax.named_scope("normwait_chip"):
+                    normed_wait(b, c)
+                normed_row(b, chips + (b // 2 - mine + chips) % chips, mate, c).start()
+
+    dn_mates(False)
+    dn_service(hz + 1, [0], "dnsvc_far0") if hz > 1 else None
     local_up.wait()
     with jax.named_scope("upwait_y"):
-        for i in range(nz):
-            up.level_wait(i)
+        for s in range(n_sp):
+            @pl.when(s % ny != y)
+            def _(s=s):
+                for c in every:
+                    up.wait(s, c)
     with jax.named_scope("normwait_mate"):
         for k in range(chips):
-            normed_wait((mate + 2 * k) % group)
+            for c in range(strips):
+                normed_wait((mate + 2 * k) % group, c)
 
     tile = min(256, half)
 
@@ -421,72 +495,118 @@
         lax.fori_loop(0, half // tile, up_tile, 0)
 
     per = max(1, 128 // cs)
-    span = ny * cs
-
-    def part(ref, at, count, zs):
+    nk = ny // per
+    span = per * cs
+
+    def part(ref, at, count, c):
         return ref.at[pl.ds(pl.multiple_of(at * rows, rows), count * rows),
-                      pl.ds(pl.multiple_of(zs * span, span), span)]
-
-    def to_mate(zs):
-        return rcopy(part(psend, (1 - core) * chips, chips, zs), part(pmate, 0, chips, zs),
-                     x_s.at[zs], x_r.at[zs], me, mate % n_tp)
-
-    def partial_to(k, zs):
-        chip = (mine + k) % chips
-        sp_to, tp_to = place(chip * 2 + core)
-        return rcopy(part(pcomb, chip, 1, zs), part(precv, mine, 1, zs), p_s.at[k * nz + zs],
-                     p_r.at[mine * nz + zs], sp_to, tp_to)
-
-    def down_level(zs):
-        for k in range(ny // per):
-            ws = [wd[zs * ny + k * per + i] for i in range(per)]
-            w = ws[0] if per == 1 else jnp.concatenate(ws, axis=1)
-            cols = pl.ds(pl.multiple_of((zs * ny + k * per) * cs, per * cs), per * cs)
-            psend[:, cols] = jnp.dot(hid[...], w, preferred_element_type=jnp.float32).astype(jnp.bfloat16)
-        to_mate(zs).start()
-
-    def combine(zs):
+                      pl.ds(pl.multiple_of(c * span, span), span)]
+
+    def to_mate(c):
+        return rcopy(part(psend, (1 - core) * chips, chips, c), part(pmate, 0, chips, c),
+                     x_s.at[c], x_r.at[c], me, mate % n_tp)
+
+    def part_beside(k, pz, c):
+        xd = (x + k) % cx
+        return rcopy(part(pcomb, pz * cx + xd, 1, c), part(precv, x * 2 + pz, 1, c), p_s.at[(k * 2 + pz) * nz * nk + c],
+                     p_r.at[(x * 2 + pz) * nz * nk + c], me, xd * 2 + core)
+
+    def part_across(c):
+        sp_to, tp_to = place(across)
+        return rcopy(part(pfar, 0, 1, c), part(pback, 0, 1, c), f_s.at[c], f_r.at[c], sp_to, tp_to)
+
+    def down_piece(c):
+        ws = [wd[c * per + i] for i in range(per)]
+        w = ws[0] if per == 1 else jnp.concatenate(ws, axis=1)
+        cols = pl.ds(pl.multiple_of(c * span, span), span)
+        m = hid.shape[0] // 2
+        for a in range(2):
+            psend[a * m:(a + 1) * m, cols] = jnp.dot(
+                hid[a * m:(a + 1) * m, :], w, preferred_element_type=jnp.float32).astype(jnp.bfloat16)
+        to_mate(c).start()
+
+    def combine(c):
         with jax.named_scope("matewait"):
-            to_mate(zs).wait_recv()
-        both = (part(psend, core * chips, chips, zs)[...].astype(jnp.float32)
-                + part(pmate, 0, chips, zs)[...].astype(jnp.float32))
-        part(pcomb, 0, chips, zs)[...] = both.astype(jnp.bfloat16)
-        for k in range(1, chips):
-            partial_to(k, zs).start()
+            to_mate(c).wait_recv()
+        both = (part(psend, core * chips, chips, c)[...].astype(jnp.float32)
+                + part(pmate, 0, chips, c)[...].astype(jnp.float32))
+        part(pcomb, 0, chips, c)[...] = both.astype(jnp.bfloat16)
+        for pz in range(2):
+            for k in range(1, cx):
+                part_beside(k, (1 - par + pz) % 2, c).start()
+
+    def reduce(c):
+        cols = pl.ds(pl.multiple_of(c * span, span), span)
+        for far in (True, False):
+            pz = 1 - par if far else par
+            total = part(pcomb, pz * cx + x, 1, c)[...].astype(jnp.float32)
+            for k in range(1, cx):
+                xs = (x + k) % cx
+                with jax.named_scope("besidewait"):
+                    rcopy(part(pcomb, 0, 1, c), part(precv, xs * 2 + pz, 1, c), p_s.at[0],
+                          p_r.at[(xs * 2 + pz) * nz * nk + c], me).wait_recv()
+                total += part(precv, xs * 2 + pz, 1, c)[...].astype(jnp.float32)
+            if far:
+                pfar[:, cols] = total.astype(jnp.bfloat16)
+                part_across(c).start()
+            else:
+                rsum[:, cols] += total
+
+    def finish(c):
+        cols = pl.ds(pl.multiple_of(c * span, span), span)
+        with jax.named_scope("acrosswait"):
+            part_across(c).wait_recv()
+        out_ref[:, cols] = (rsum[:, cols] + pback[:, cols].astype(jnp.float32)).astype(jnp.bfloat16)
 
     local_dn.wait()
+
+    @pl.when(par == 1)
+    def _():
+        dn_service(hz, range(1, cuts), "dnsvc_part1")
+    late = [(hz + 1, c) for c in range(1, cuts)] + [(i, c) for i in range(hz + 2, nz) for c in every]
+    pieces = []
     for i in range(nz):
-        if i + 1 < nz:
-            with jax.named_scope("dnwait_z"):
-                dn.service(i + 1)
-        with jax.named_scope("dnwait_y"):
-            dn.level_wait(i)
-        with jax.named_scope("down_mm"):
-            down_level(dn.order(i))
-        if i > 0:
-            combine(dn.order(i - 1))
-    combine(dn.order(nz - 1))
-
-    total = rsum[...]
-    whole_row = lambda ref, at: ref[pl.ds(pl.multiple_of(at * rows, rows), rows), :].astype(jnp.float32)
-    total += whole_row(pcomb, mine)
-    for k in range(1, chips):
-        src = (mine + k) % chips
-        with jax.named_scope("partwait"):
-            for zs in range(nz):
-                rcopy(part(pcomb, src, 1, zs), part(precv, src, 1, zs), p_s.at[0], p_r.at[src * nz + zs], me).wait_recv()
-        total += whole_row(precv, src)
-    out_ref[...] = total.astype(jnp.bfloat16)
+        zs = dn.order(i)
+        for k in range(nk):
+            c = zs * nk + (y // per + k) % nk
+            if i >= hz - 1 and k == 0:
+                for j, cut in [t for t in late if t[0] == i + 1]:
+                    dn_service(j, [cut], "dnsvc_far")
+            with jax.named_scope("dnwait_y"):
+                for o in range(per):
+                    s = c * per + o
+
+                    @pl.when(s % ny != y)
+                    def _(s=s):
+                        for cut in every:
+                            dn.wait(s, cut)
+            with jax.named_scope("down_mm"):
+                down_piece(c)
+            pieces.append(c)
+            n = len(pieces)
+            if n > 1:
+                combine(pieces[n - 2])
+            if n > 3:
+                reduce(pieces[n - 4])
+    n = len(pieces)
+    combine(pieces[n - 1])
+    for c in pieces[max(0, n - 3):]:
+        reduce(c)
+    for c in pieces:
+        finish(c)
 
     for dy in range(1, ny):
         @pl.when(keys_wanted(dy))
         def _(dy=dy):
             for c in keys_to(dy):
                 c.wait_send()
-    for zk in range(nz - 1):
-        @pl.when(zk < z)
-        def _(zk=zk):
-            query_to(zk).wait_send()
+    @pl.when(z > 0)
+    def _():
+        query_first().wait_send()
+    for zq in range(2, nz):
+        @pl.when((zq > z) & (z > 0))
+        def _(zq=zq):
+            query_on(zq).wait_send()
     for zq in range(1, nz):
         @pl.when(zq > z)
         def _(zq=zq):
@@ -496,16 +616,19 @@
     dn.drain()
     for o in range(1, n_tp):
         heads_to(o).wait_send()
-    normed_across().wait_send()
-    for k in range(1, cx):
-        normed_beside(k).wait_send()
-        normed_relay(k).wait_send()
-    for k in range(chips):
-        normed_mate(k).wait_send()
-    for zs in range(nz):
-        to_mate(zs).wait_send()
-        for k in range(1, chips):
-            partial_to(k, zs).wait_send()
+    for c in range(strips):
+        normed_across(c).wait_send()
+        for k in range(1, cx):
+            normed_beside(k, c).wait_send()
+            normed_relay(k, c).wait_send()
+        for k in range(chips):
+            normed_mate(k, c).wait_send()
+    for c in range(nz * nk):
+        to_mate(c).wait_send()
+        part_across(c).wait_send()
+        for pz in range(2):
+            for k in range(1, cx):
+                part_beside(k, pz, c).wait_send()
 
 
 def per_device(n_sp, n_tp, queries, keys, values, cum_gate, residual, w_out, gain, w_up, w_down):
@@ -524,6 +647,7 @@
     hbm = pl.BlockSpec(memory_space=pl.ANY)
     dma = lambda n: pltpu.SemaphoreType.DMA((n,))
     lanes = max(128, nz * STAT)
+    pieces = nz * (ny // max(1, 128 // w_down.shape[1]))
     return pl.pallas_call(
         functools.partial(body, n_sp, n_tp, heads),
         out_shape=jax.ShapeDtypeStruct((rows, features), bf),
@@ -554,10 +678,13 @@
             pltpu.VMEM((n_tp * rows, features), bf),
             pltpu.VMEM((n_tp * rows, features), bf),
             pltpu.VMEM((n_tp * rows, features), bf),
+            pltpu.VMEM((rows, features), bf),
+            pltpu.VMEM((rows, features), bf),
         ]
         + [dma(nz), dma(nz)] + [dma(ny)] * 6 + [dma(nz)] * 4
-        + [dma(hz), dma(hz), dma(n_sp), dma(n_sp)] * 2
-        + [dma(n_tp), dma(n_tp), dma(group + n_tp), dma(group), dma(n_tp * nz), dma(n_tp * nz), dma(nz), dma(nz), dma(3)],
+        + [dma(hz * CUTS), dma(hz * CUTS), dma(n_sp * CUTS), dma(n_sp * CUTS)] * 2
+        + [dma(n_tp), dma(n_tp), dma(2 * group), dma(2 * group)]
+        + [dma(n_tp * pieces), dma(n_tp * pieces)] + [dma(pieces)] * 4 + [dma(3)],
         compiler_params=pltpu.CompilerParams(
             collective_id=0, has_side_effects=True, vmem_limit_bytes=63 * 1024 * 1024
         ),

time: 176 us -> 146 us (0.83); the launches traced: 173 us -> 146 us
  Pallas kernels: 170 us -> 142 us
    pallas_call x1, Pallas kernels: 170 us -> 142 us  [per_device(): pl.pallas_call(functools.partial(body, n_sp, n_tp, heads), out_shape=jax....]
where the time goes in v2:
time: 146 us
  Pallas kernels  142 us (97%)
  local copies, waits for them, and re-layouts  3.18 us (2%)
    pallas_call x1, Pallas kernels, per_device(): pl.pallas_call(functools.partial(body, n_sp, n_tp, heads), out_shape=jax....  142 us

profile of v2, /device:TPU:0, one launch (start us, length us, event | category | flops | bytes accessed | tf_op | source)
XLA Modules:
  0.0 145.6 jit_solution(16319431468482704593)
XLA Ops:
  0.0 1.3 pad.4.gate_ref
  1.3 142.4 %shard_map.91 = bf16[128,2048]{1,0:T(8,128)(2,1)} custom-call(bf16[512,256]{1,0:T(8,128)(2,1)} %q_ref.1, bf16[512,256]{1,0:T(8,128)(2,1)} %k_ref.1, bf16[512,256]{1,0:T(8,128)(2,1)} %v_ref.1, f32[8,512]{1,0:T(8,128)} %pad.4.gate_ref, bf16[128,2048]{1,0:T(8,128)(2,1)} %res_ref.1, bf16[1024,2048]{1,0:T(8,128)(2,1)} %wout_hbm.1, f32[1,2048]{1,0:T(1,128)} %bitcast.2, ...), custom_call_target="tpu_custom_call" | custom-call | tf_op jit(solution)/shard_map/pallas_call | solution.py:651
  143.7 1.9 %copy.11 = bf16[128,2048]{1,0:T(8,128)(2,1)} copy(bf16[128,2048]{1,0:T(8,128)(2,1)} %shard_map.91) | data formatting | bytes 1048576

commit v3 on v2

--- a/solution.py
+++ b/solution.py
@@ -11,7 +11,26 @@
 LOG2E = math.log2(math.e)
 NEG = -1e30
 STAT = 8
-CUTS = 2
+
+
+PLAN = dict(
+    up_part=[0, 0, 2, 2],
+    up_mate=[2, 1, 0, 1],
+    dn_part0=[4, 2, 3, 3],
+    dn_part1=[6, 6, 5, 6],
+    dn_mate=[6, 5, 5, 5],
+    s_up_mate=[1, 1, 0, 0],
+    s_part0=[2, 2, 3, 3],
+    s_part1=[5, 5, 5, 5],
+    s_mate=[5, 5, 3, 5],
+    s_far0=[5, 5, 5, 5],
+    gates=[1, 0],
+    style=[1],
+    lag=[3],
+    cuts=[4],
+    strips=[4],
+    own_y=[0],
+)
 
 
 class Weights:
@@ -90,11 +109,11 @@
     n_sp, n_tp, heads,
     q_ref, k_ref, v_ref, gate_ref, res_ref, wout_hbm, gain_ref, wup_hbm, wdn_hbm,
     out_ref,
-    q_all, k_all, v_all, g_all, o_send, o_recv, t_send, t_recv, st_s, m_s, l_s, acc_s,
+    q_all, k_all, v_all, g_all, o_send, o_recv, t_send, t_recv, o_mid, t_mid, t_own, st_s, m_s, l_s, acc_s,
     att, att_in, wout, rsum, wu, wd, norm_all, hid, psend, pmate, pcomb, precv, pfar, pback,
-    q_s, q_r, k_s, k_r, v_s, v_r, g_s, g_r, o_s, o_r, t_s, t_r,
+    q_s, q_r, k_s, k_r, v_s, v_r, g_s, g_r, o_s, o_r, t_s, t_r, om_r, tm_r,
     u_z, u_l, u_y, u_r, d_z, d_l, d_y, d_r,
-    a_s, a_r, n_s, n_r, p_s, p_r, x_s, x_r, f_s, f_r, loc,
+    a_s, a_r, n_s, n_r, p_s, p_r, x_s, x_r, f_s, f_r, loc, go,
 ):
     ny = n_tp // 2
     nz = n_sp // ny
@@ -132,10 +151,16 @@
     g_all[pl.ds(y, 1)] = gate_ref[...][None]
     st_s[...] = jnp.zeros_like(st_s)
     t_recv[...] = jnp.zeros_like(t_recv)
+    t_mid[...] = jnp.zeros_like(t_mid)
+    t_own[...] = jnp.zeros_like(t_own)
 
     barrier = pltpu.get_barrier_semaphore()
+    far_mates = [(s, mate % n_tp) for j in range(1, hz) for s in [(par * hz + (zi + j) % hz) * ny + y]]
     for dz in range(1, nz):
         pl.semaphore_signal(barrier, inc=1, device_id={"sp": ((z + dz) % nz) * ny + y},
+                            device_id_type=pl.DeviceIdType.MESH)
+    for sp_to, tp_to in far_mates:
+        pl.semaphore_signal(barrier, inc=1, device_id={"sp": sp_to, "tp": tp_to},
                             device_id_type=pl.DeviceIdType.MESH)
     for dy in range(1, ny):
         pl.semaphore_signal(barrier, inc=1, device_id={"sp": z * ny + (y + dy) % ny},
@@ -145,11 +170,11 @@
         pl.semaphore_signal(barrier, inc=1, device_id={"sp": sp_to, "tp": tp_to},
                             device_id_type=pl.DeviceIdType.MESH)
     with jax.named_scope("bar"):
-        pl.semaphore_wait(barrier, nz - 1 + ny - 1 + group - 1)
+        pl.semaphore_wait(barrier, nz - 1 + hz - 1 + ny - 1 + group - 1)
 
     geo = Geo()
     geo.nz, geo.ny, geo.hz, geo.me, geo.z, geo.y, geo.par, geo.zi = nz, ny, hz, me, z, y, par, zi
-    cuts = CUTS
+    cuts = PLAN["cuts"][0]
     upc, dnc = up_rows // cuts, half // cuts
     up = Weights(
         geo, cuts, rcopy,
@@ -173,20 +198,47 @@
     def keys_wanted(dy):
         return (z + 1 < nz) | ((y + dy) % ny > y)
 
-    def query_first():
-        return rcopy(q_ref, q_all.at[z], q_s.at[z], q_r.at[z], me - ny)
-
-    def query_on(zq):
-        return rcopy(q_all.at[zq], q_all.at[zq], q_s.at[zq], q_r.at[zq], me - ny)
-
-    def query_wait(zq):
-        rcopy(q_ref, q_all.at[zq], q_s.at[0], q_r.at[zq], me).wait_recv()
+    def query_head(src, zq, h):
+        cols = pl.ds(h * hd, hd)
+        return rcopy(src.at[:, cols], q_all.at[zq, :, cols], q_s.at[zq * heads + h], q_r.at[zq * heads + h], me - ny)
+
+    def query_first(h):
+        return query_head(q_ref, z, h)
+
+    def query_on(zq, h):
+        return query_head(q_all.at[zq], zq, h)
+
+    def query_wait(zq, h):
+        cols = pl.ds(h * hd, hd)
+        rcopy(q_ref.at[:, cols], q_all.at[zq, :, cols], q_s.at[0], q_r.at[zq * heads + h], me).wait_recv()
+
+    def part_copies(zq, o_to, t_to, at, o_sem, t_sem, to):
+        rows_at = pl.ds(pl.multiple_of(at * STAT, STAT), STAT)
+        return (rcopy(o_send.at[zq], o_to.at[at], o_s.at[zq], o_sem.at[at], to),
+                rcopy(t_send.at[zq], t_to.at[rows_at, :], t_s.at[zq], t_sem.at[at], to))
 
     def part_to(zq):
-        to = zq * ny + y
-        at = pl.ds(pl.multiple_of(z * STAT, STAT), STAT)
-        return (rcopy(o_send.at[zq], o_recv.at[z], o_s.at[zq], o_r.at[z], to),
-                rcopy(t_send.at[zq], t_recv.at[at, :], t_s.at[zq], t_r.at[z], to))
+        return part_copies(zq, o_recv, t_recv, z, o_r, t_r, zq * ny + y)
+
+    def part_inward(zq):
+        return part_copies(zq, o_mid, t_mid, zq, om_r, tm_r, me + ny)
+
+    def inward(zq):
+        return (par == 0) & (zq >= hz) & (zi < hz - 1)
+
+    def merged(zq):
+        return (par == 0) & (zq >= hz) & (zi > 0)
+
+    def part_do(zq, do):
+        @pl.when(inward(zq))
+        def _():
+            for c in part_inward(zq):
+                do(c)
+
+        @pl.when(jnp.logical_not(inward(zq)))
+        def _():
+            for c in part_to(zq):
+                do(c)
 
     for dy in range(1, ny):
         @pl.when(keys_wanted(dy))
@@ -195,7 +247,8 @@
                 c.start()
     @pl.when(z > 0)
     def _():
-        query_first().start()
+        for h in range(heads):
+            query_first(h).start()
     local_wout = pltpu.make_async_copy(wout_hbm, wout, loc.at[0])
     local_up = pltpu.make_async_copy(
         wup_hbm.at[:, pl.ds(pl.multiple_of(par * half, half), half)],
@@ -203,29 +256,48 @@
     local_dn = pltpu.make_async_copy(
         wdn_hbm.at[pl.ds(pl.multiple_of(par * half, half), half), :], wd.at[me], loc.at[2])
 
-    def direct_mates(w, upward):
+    every = range(cuts)
+    first, rest = range(cuts // 2), range(cuts // 2, cuts)
+    kind = jnp.where(par == 0, jnp.where(zi == hz - 1, 1, 0), jnp.where(zi == 0, 2, 3))
+
+    def at_kinds(places, now, act):
+        for q in range(4):
+            if places[q] == now:
+                @pl.when(kind == q)
+                def _():
+                    act()
+
+    def partner(w, chunks):
+        for c in chunks:
+            w.to_partner(c).start()
+
+    def mates(w):
         for j in range(1, hz):
-            @pl.when((w.mate(j) > z) if upward else (w.mate(j) < z))
-            def _(j=j):
-                for c in range(cuts):
-                    w.to_mate(j, c).start()
-
-    def direct_partner(w, upward, chunks):
-        @pl.when(par == (0 if upward else 1))
-        def _():
-            for c in chunks:
-                w.to_partner(c).start()
-
-    every = range(cuts)
-    direct_partner(up, True, every)
-    direct_mates(up, True)
+            for c in every:
+                w.to_mate(j, c).start()
+
+    def issue(slot):
+        at_kinds(PLAN["up_part"], slot, lambda: partner(up, every))
+        at_kinds(PLAN["up_mate"], slot, lambda: mates(up))
+        at_kinds(PLAN["dn_part0"], slot, lambda: partner(dn, first))
+        at_kinds(PLAN["dn_part1"], slot, lambda: partner(dn, rest))
+        at_kinds(PLAN["dn_mate"], slot, lambda: mates(dn))
+        if slot > 0 and PLAN["own_y"][0] == slot:
+            beside_y(dn)
+
+    issue(0)
     local_up.start()
     local_dn.start()
     local_wout.start()
-    for w in (up, dn):
+
+    def beside_y(w):
         for dy in range(1, ny):
             for c in every:
                 w.own_y(dy, c).start()
+
+    beside_y(up)
+    if PLAN["own_y"][0] == 0:
+        beside_y(dn)
 
     scale = hd ** (-0.5) * LOG2E
 
@@ -274,7 +346,9 @@
             o_send[zq, :, cols] = add.astype(jnp.bfloat16)
             st_s[:, h:h + 1] = top - base
             st_s[:, heads + h:heads + h + 1] = total
-        t_send[zq] = jnp.transpose(st_s[...])[0:STAT, :]
+        stats = jnp.transpose(st_s[...])[0:STAT, :]
+        t_send[zq] = stats
+        t_own[pl.ds(pl.multiple_of(zq * STAT, STAT), STAT), :] = stats
 
     with jax.named_scope("diag"):
         absorb(k_ref, v_ref, gate_ref, True)
@@ -282,11 +356,11 @@
     for zq in range(2, nz):
         @pl.when((zq > z) & (z > 0))
         def _(zq=zq):
-            with jax.named_scope("qfwd"):
-                query_wait(zq)
-            query_on(zq).start()
-    direct_mates(up, False)
-    direct_partner(up, False, every)
+            for h in range(heads):
+                with jax.named_scope("qfwd"):
+                    query_wait(zq, h)
+                query_on(zq, h).start()
+    issue(1)
 
     for dy in range(1, ny):
         src = (y + dy) % ny
@@ -310,28 +384,69 @@
             @pl.when(z == 0)
             def _():
                 with jax.named_scope("qwait"):
-                    query_wait(zq)
+                    for h in range(heads):
+                        query_wait(zq, h)
             with jax.named_scope("partial"):
                 partial(zq)
-            for c in part_to(zq):
-                c.start()
+
+            @pl.when(jnp.logical_not(merged(zq)))
+            def _():
+                part_do(zq, lambda c: c.start())
         return carry
 
     lax.fori_loop(0, nz - 1, query_level, 0)
-
-    with jax.named_scope("upsvc"):
-        for i in [hz] + list(range(1, hz)):
-            for c in every:
-                up.service(i, c)
-    direct_partner(dn, False, every)
-    direct_partner(dn, True, [0])
-    for p in range(2):
-        @pl.when(par == p)
-        def _(p=p):
-            direct_mates(dn, p == 1)
+    issue(2)
+
+    for zq in range(hz, nz):
+        @pl.when(merged(zq))
+        def _(zq=zq):
+            rows_at = pl.ds(zq * STAT, STAT)
+            with jax.named_scope("midwait"):
+                rcopy(o_send.at[0], o_mid.at[zq], o_s.at[0], om_r.at[zq], me).wait_recv()
+                rcopy(t_send.at[0], t_mid.at[rows_at, :], t_s.at[0], tm_r.at[zq], me).wait_recv()
+            t_own[0:STAT, :] = t_mid[rows_at, :]
+            both = jnp.transpose(t_own[...])
+            for h in range(heads):
+                cols = pl.ds(h * hd, hd)
+                at = zq * STAT + h
+                m1, l1 = both[:, at:at + 1], both[:, at + heads:at + heads + 1]
+                m2, l2 = both[:, h:h + 1], both[:, heads + h:heads + h + 1]
+                top = jnp.maximum(m1, m2)
+                f1, f2 = jnp.exp2(m1 - top), jnp.exp2(m2 - top)
+                o_send[zq, :, cols] = (o_send[zq, :, cols].astype(jnp.float32) * f1
+                                       + o_mid[zq, :, cols].astype(jnp.float32) * f2).astype(jnp.bfloat16)
+                st_s[:, h:h + 1] = top
+                st_s[:, heads + h:heads + h + 1] = l1 * f1 + l2 * f2
+            t_send[zq] = jnp.transpose(st_s[...])[0:STAT, :]
+            part_do(zq, lambda c: c.start())
+
+    def serve(w, i, chunks, name):
+        for c in chunks:
+            with jax.named_scope(name):
+                w.service(i, c)
+
+    def up_mates():
+        for j in range(1, hz):
+            serve(up, j, every, "upsvc_mate")
+
+    def early_up():
+        serve(up, hz, every, "upsvc_part")
+
+        at_kinds(PLAN["s_up_mate"], 0, up_mates)
+        issue(3)
+    def pass_on(when):
+        at_kinds(PLAN["s_part0"], when, lambda: serve(dn, hz, first, "dnsvc_part0"))
+        at_kinds(PLAN["s_part1"], when, lambda: serve(dn, hz, rest, "dnsvc_part1"))
+        for j in range(1, hz):
+            at_kinds(PLAN["s_mate"], when, lambda: serve(dn, j, every, "dnsvc_mate"))
+            at_kinds(PLAN["s_far0"], when, lambda: serve(dn, hz + j, first, "dnsvc_far0"))
+
+    @pl.when(z > 0)
+    def _():
+        early_up()
 
     for zk in range(nz - 1):
-        @pl.when(zk < z)
+        @pl.when((zk < z) & ((par == 0) | (zk >= hz - 1)))
         def _(zk=zk):
             with jax.named_scope("owait"):
                 at = pl.ds(zk * STAT, STAT)
@@ -343,7 +458,7 @@
         st_s[...] = jnp.transpose(t_recv[...])
 
     for zk in range(nz - 1):
-        @pl.when(zk < z)
+        @pl.when((zk < z) & ((par == 0) | (zk >= hz - 1)))
         def _(zk=zk):
             for h in range(heads):
                 cols = pl.ds(h * hd, hd)
@@ -386,7 +501,7 @@
         return ref.at[pl.ds(pl.multiple_of(at * rows, rows), rows), :]
 
     block(norm_all, slot)[...] = normed
-    strips = 2
+    strips = PLAN["strips"][0]
     strip = norm_all.shape[1] // strips
 
     def strip_of(b, c):
@@ -417,43 +532,44 @@
     def normed_wait(src, c):
         rcopy(strip_of(src, c), strip_of(src, c), n_s.at[0], n_r.at[src * strips + c], me).wait_recv()
 
-    for c in range(strips):
-        normed_across(c).start()
+    def gate(g):
+        outer = jnp.where(par == 0, zi, hz - 1 - zi)
+        for i in range(hz - 1):
+            @pl.when(i < outer)
+            def _(i=i):
+                to = par * hz + jnp.where(par == 0, i, hz - 1 - i)
+                for t in (tp, mate % n_tp):
+                    pl.semaphore_signal(go.at[g], inc=1, device_id={"sp": to * ny + y, "tp": t},
+                                        device_id_type=pl.DeviceIdType.MESH)
+        pl.semaphore_signal(go.at[g], inc=1, device_id={"tp": mate % n_tp}, device_id_type=pl.DeviceIdType.MESH)
+        with jax.named_scope("gate"):
+            pl.semaphore_wait(go.at[g], 2 * (hz - 1 - outer) + 1)
+
     for c in range(strips):
         for k in range(1, cx):
             normed_beside(k, c).start()
     for c in range(strips):
         normed_mate(0, c).start()
-    direct_partner(dn, True, range(1, cuts))
-    for p in range(2):
-        @pl.when(par == p)
-        def _(p=p):
-            direct_mates(dn, p == 0)
-
-    with jax.named_scope("upsvc2"):
-        for i in range(hz + 1, nz):
-            for c in every:
-                up.service(i, c)
-
-    def dn_service(i, chunks, name):
-        for c in chunks:
-            with jax.named_scope(name):
-                dn.service(i, c)
-
-    def dn_mates(soon):
-        for j in range(1, hz):
-            zs = dn.mate(j)
-
-            @pl.when((zs < z) == ((par == 1) == soon))
-            def _(j=j):
-                dn_service(j, every, "dnsvc_mate")
-
-    dn_service(hz, [0], "dnsvc_part0")
-
-    @pl.when(par == 0)
+
+    @pl.when(z == 0)
     def _():
-        dn_service(hz, range(1, cuts), "dnsvc_part1")
-    dn_mates(True)
+        early_up()
+    for zq in range(1, nz):
+        @pl.when(zq > z)
+        def _(zq=zq):
+            with jax.named_scope("osent"):
+                part_do(zq, lambda c: c.wait_send())
+    if PLAN["gates"][0]:
+        gate(0)
+    issue(4)
+    for c in range(strips):
+        normed_across(c).start()
+    issue(5)
+    at_kinds(PLAN["s_up_mate"], 1, up_mates)
+    pass_on(1)
+    for j in range(1, hz):
+        serve(up, hz + j, every, "upsvc_far")
+    pass_on(2)
 
     for c in range(strips):
         with jax.named_scope("normwait_across"):
@@ -461,6 +577,13 @@
         for k in range(1, cx):
             normed_relay(k, c).start()
         normed_mate(chips // 2, c).start()
+    with jax.named_scope("e2sent"):
+        for c in range(strips):
+            normed_across(c).wait_send()
+    if PLAN["gates"][1]:
+        gate(1)
+    issue(6)
+    pass_on(3)
     for near in (True, False):
         for k in range(1, cx):
             for c in range(strips):
@@ -469,8 +592,6 @@
                     normed_wait(b, c)
                 normed_row(b, chips + (b // 2 - mine + chips) % chips, mate, c).start()
 
-    dn_mates(False)
-    dn_service(hz + 1, [0], "dnsvc_far0") if hz > 1 else None
     local_up.wait()
     with jax.named_scope("upwait_y"):
         for s in range(n_sp):
@@ -560,38 +681,58 @@
 
     local_dn.wait()
 
-    @pl.when(par == 1)
-    def _():
-        dn_service(hz, range(1, cuts), "dnsvc_part1")
-    late = [(hz + 1, c) for c in range(1, cuts)] + [(i, c) for i in range(hz + 2, nz) for c in every]
     pieces = []
-    for i in range(nz):
-        zs = dn.order(i)
-        for k in range(nk):
-            c = zs * nk + (y // per + k) % nk
-            if i >= hz - 1 and k == 0:
-                for j, cut in [t for t in late if t[0] == i + 1]:
-                    dn_service(j, [cut], "dnsvc_far")
-            with jax.named_scope("dnwait_y"):
-                for o in range(per):
-                    s = c * per + o
-
-                    @pl.when(s % ny != y)
-                    def _(s=s):
-                        for cut in every:
-                            dn.wait(s, cut)
-            with jax.named_scope("down_mm"):
-                down_piece(c)
-            pieces.append(c)
-            n = len(pieces)
-            if n > 1:
-                combine(pieces[n - 2])
-            if n > 3:
-                reduce(pieces[n - 4])
-    n = len(pieces)
-    combine(pieces[n - 1])
-    for c in pieces[max(0, n - 3):]:
-        reduce(c)
+    done = [0, 0]
+
+    def flush(upto, summed):
+        while done[0] < upto:
+            combine(pieces[done[0]])
+            done[0] += 1
+        while done[1] < summed:
+            reduce(pieces[done[1]])
+            done[1] += 1
+
+    def piece(i, k):
+        c = dn.order(i) * nk + (y // per + k) % nk
+        with jax.named_scope("dnwait_y"):
+            for o in range(per):
+                s = c * per + o
+
+                @pl.when(s % ny != y)
+                def _(s=s):
+                    for cut in every:
+                        dn.wait(s, cut)
+        with jax.named_scope("down_mm"):
+            down_piece(c)
+        pieces.append(c)
+        flush(len(pieces) - 1, len(pieces) - PLAN["lag"][0])
+
+    for k in range(nk):
+        piece(0, k)
+    if PLAN["style"][0] == 0:
+        pass_on(5)
+    else:
+        at_kinds(PLAN["s_part0"], 5, lambda: serve(dn, hz, first, "dnsvc_part0"))
+        at_kinds(PLAN["s_part1"], 5, lambda: serve(dn, hz, rest, "dnsvc_part1"))
+        piece(hz, 0)
+    for j in range(1, hz):
+        if PLAN["style"][0] == 1:
+            at_kinds(PLAN["s_mate"], 5, lambda: serve(dn, j, every, "dnsvc_mate"))
+            at_kinds(PLAN["s_far0"], 5, lambda: serve(dn, hz + j, first, "dnsvc_far0"))
+        piece(j, 0)
+    if PLAN["style"][0] == 0:
+        piece(hz, 0)
+    for j in range(1, hz):
+        serve(dn, hz + j, rest, "dnsvc_far")
+        if PLAN["style"][0] == 1:
+            piece(hz + j, 0)
+    for k in range(1, nk):
+        for i in ([hz] + list(range(1, hz)) if PLAN["style"][0] == 1 else list(range(1, hz)) + [hz]):
+            piece(i, k)
+    for j in range(1, hz):
+        for k in range(PLAN["style"][0], nk):
+            piece(hz + j, k)
+    flush(len(pieces), len(pieces))
     for c in pieces:
         finish(c)
 
@@ -602,22 +743,18 @@
                 c.wait_send()
     @pl.when(z > 0)
     def _():
-        query_first().wait_send()
+        for h in range(heads):
+            query_first(h).wait_send()
     for zq in range(2, nz):
         @pl.when((zq > z) & (z > 0))
         def _(zq=zq):
-            query_on(zq).wait_send()
-    for zq in range(1, nz):
-        @pl.when(zq > z)
-        def _(zq=zq):
-            for c in part_to(zq):
-                c.wait_send()
+            for h in range(heads):
+                query_on(zq, h).wait_send()
     up.drain()
     dn.drain()
     for o in range(1, n_tp):
         heads_to(o).wait_send()
     for c in range(strips):
-        normed_across(c).wait_send()
         for k in range(1, cx):
             normed_beside(k, c).wait_send()
             normed_relay(k, c).wait_send()
@@ -642,7 +779,7 @@
     half = w_up.shape[1] // 2
     bf, f32 = jnp.bfloat16, jnp.float32
     assert nz % 2 == 0 and 2 * heads <= STAT
-    gates = jnp.pad(cum_gate.T, ((0, 8 - heads), (0, 0)))
+    gates = cum_gate.T
     vmem = pl.BlockSpec(memory_space=pltpu.VMEM)
     hbm = pl.BlockSpec(memory_space=pl.ANY)
     dma = lambda n: pltpu.SemaphoreType.DMA((n,))
@@ -661,6 +798,9 @@
             pltpu.VMEM((nz, tok, width), bf),
             pltpu.VMEM((nz, tok, width), bf),
             pltpu.VMEM((nz, STAT, tok), f32),
+            pltpu.VMEM((lanes, tok), f32),
+            pltpu.VMEM((nz, tok, width), bf),
+            pltpu.VMEM((lanes, tok), f32),
             pltpu.VMEM((lanes, tok), f32),
             pltpu.VMEM((tok, lanes), f32),
             pltpu.VMEM((tok, 128), f32),
@@ -681,10 +821,10 @@
             pltpu.VMEM((rows, features), bf),
             pltpu.VMEM((rows, features), bf),
         ]
-        + [dma(nz), dma(nz)] + [dma(ny)] * 6 + [dma(nz)] * 4
-        + [dma(hz * CUTS), dma(hz * CUTS), dma(n_sp * CUTS), dma(n_sp * CUTS)] * 2
-        + [dma(n_tp), dma(n_tp), dma(2 * group), dma(2 * group)]
-        + [dma(n_tp * pieces), dma(n_tp * pieces)] + [dma(pieces)] * 4 + [dma(3)],
+        + [dma(nz * heads)] * 2 + [dma(ny)] * 6 + [dma(nz)] * 6
+        + [dma(hz * PLAN["cuts"][0]), dma(hz * PLAN["cuts"][0]), dma(n_sp * PLAN["cuts"][0]), dma(n_sp * PLAN["cuts"][0])] * 2
+        + [dma(n_tp), dma(n_tp), dma(PLAN["strips"][0] * group), dma(PLAN["strips"][0] * group)]
+        + [dma(n_tp * pieces), dma(n_tp * pieces)] + [dma(pieces)] * 4 + [dma(3), pltpu.SemaphoreType.REGULAR((2,))],
         compiler_params=pltpu.CompilerParams(
             collective_id=0, has_side_effects=True, vmem_limit_bytes=63 * 1024 * 1024
         ),

time: 146 us -> 140 us (0.959)
  Pallas kernels: 142 us -> 138 us
    pallas_call x1, Pallas kernels: 142 us -> 138 us  [per_device(): pl.pallas_call(functools.partial(body, n_sp, n_tp, heads), out_shape=jax....]
where the time goes in v3:
time: 140 us
  Pallas kernels  138 us (99%)
  local copies, waits for them, and re-layouts  1.88 us (1%)
    pallas_call x1, Pallas kernels, per_device(): pl.pallas_call(functools.partial(body, n_sp, n_tp, heads), out_shape=jax....  138 us

profile of v3, /device:TPU:0, one launch (start us, length us, event | category | flops | bytes accessed | tf_op | source)
XLA Modules:
  0.0 139.6 jit_solution(4707141983104236398)
XLA Ops:
  0.0 137.7 %shard_map.91 = bf16[128,2048]{1,0:T(8,128)(2,1)} custom-call(bf16[512,256]{1,0:T(8,128)(2,1)} %q_ref.1, bf16[512,256]{1,0:T(8,128)(2,1)} %k_ref.1, bf16[512,256]{1,0:T(8,128)(2,1)} %v_ref.1, f32[2,512]{1,0:T(2,128)} %bitcast.3, bf16[128,2048]{1,0:T(8,128)(2,1)} %res_ref.1, bf16[1024,2048]{1,0:T(8,128)(2,1)} %wout_hbm.1, f32[1,2048]{1,0:T(1,128)} %bitcast.2, ...), custom_call_target="tpu_custom_call" | custom-call | tf_op jit(solution)/shard_map/pallas_call | solution.py:788
  137.7 1.9 %copy.11 = bf16[128,2048]{1,0:T(8,128)(2,1)} copy(bf16[128,2048]{1,0:T(8,128)(2,1)} %shard_map.91) | data formatting | bytes 1048576
